TPU v7x, 128 devices: a whole 4x4x4 slice. The times are simulated.
128 devices in a mesh: sp: 16 (over z, y), tp: 8 (over x, core).
Axes of the slice: x: 4, y: 4, z: 4, core: 2. Of those that a mesh axis runs over, the one named last changes fastest.
Arguments:
- queries: bfloat16 [12288, 2048], P('sp', 'tp'), may hold values from -11 to 11
- key_rows: bfloat16 [12288, 2048], P('sp', 'tp'), may hold values from -4.5 to 4.5
- value_rows: bfloat16 [12288, 2048], P('sp', 'tp'), may hold values from -6 to 6
- log_forget: float32 [12288, 32], P('sp', 'tp'), may hold values from -1477.56 to 0, as said below
- stream_in: bfloat16 [12288, 2048], P('sp'), may hold values from -6 to 6
- out_weight: bfloat16 [2048, 2048], P('tp'), may hold values from -0.52734375 to 0.52734375
- mix_gain: float32 [2048], replicated, may hold values from 0.1 to 1.9
- mix_bias: float32 [2048], replicated, may hold values from -3 to 3
- gate_weight: bfloat16 [2048, 5632], P('sp', 'tp'), may hold values from -0.125 to 0.125
- up_weight: bfloat16 [2048, 5632], P('sp', 'tp'), may hold values from -0.125 to 0.125
- down_weight: bfloat16 [5632, 2048], P('tp', 'sp'), may hold values from -0.15917969 to 0.15917969
- ffn_gain: float32 [2048], replicated, may hold values from 0.1 to 1.9
- ffn_bias: float32 [2048], replicated, may hold values from -3 to 3
Outputs:
- layer_out: bfloat16 [12288, 2048], P(('sp', 'tp'))
Inputs may be any that keep to these rules, and one draw needn't show every extreme that they name: `log_forget`: each column never rises along the positions.
All inputs are finite; a program needn't handle non-finite values.
Results may differ from a plain program's by a relative error of at most 0.015.
Values may be sent and summed in bfloat16 or wider, within the bound.
A program may use at most 128 MiB of HBM per device.

v0:
```python
import jax
import jax.numpy as jnp
from jax import lax
from jax.sharding import PartitionSpec as P

ALPHA = 8.0**0.25
EPSILON = 1e-05


def laid_out(pieces, dim):
    lengths = list(pieces.shape[1:])
    lengths[dim] *= pieces.shape[0]
    return jnp.moveaxis(pieces, 0, dim).reshape(lengths)


def from_everyone(value, axis):
    copies = jnp.broadcast_to(value, (lax.axis_size(axis), *value.shape))
    return lax.all_to_all(copies, axis, split_axis=0, concat_axis=0, tiled=True)


def gathered_copies(value, axis, dim):
    return laid_out(from_everyone(value, axis), dim)


def in_one_piece(arrays, axis, dim, along):
    ends, at = ([], 0)
    for a in arrays[:-1]:
        at += a.shape[along]
        ends.append(at)
    both = jnp.concatenate(arrays, axis=along)
    return tuple(jnp.split(lax.all_gather(both, axis, axis=dim, tiled=True), ends, axis=along))


def in_blocks(value, dim, count):
    before, after = (value.shape[:dim], value.shape[dim + 1 :])
    return jnp.moveaxis(value.reshape(*before, count, -1, *after), dim, 0)


def sum_at_owner(value, axis, dim):
    pieces = in_blocks(value, dim, lax.axis_size(axis))
    arrived = lax.all_to_all(pieces, axis, split_axis=0, concat_axis=0, tiled=True)
    return arrived.astype(jnp.float32).sum(axis=0)


def layer_norm(matrix, norm_gain, norm_shift):
    centred = matrix - jnp.mean(matrix, axis=-1, keepdims=True)
    spread = jnp.mean(centred * centred, axis=-1, keepdims=True)
    return centred * lax.rsqrt(spread + EPSILON) * norm_gain + norm_shift


def attend(queries, key_rows, value_rows, log_forget):
    length, row_width = queries.shape
    head_count = log_forget.shape[1]
    head_dim = row_width // head_count
    score_scale = head_dim ** (-0.5)
    first_pos = lax.axis_index("sp") * length
    last_pos = first_pos + length
    query_heads = queries.reshape(length, head_count, head_dim)
    query_gates = log_forget.T
    query_pos = first_pos + jnp.arange(length, dtype=jnp.int32)
    gates_all = gathered_copies(log_forget, "sp", 0)
    initial = (
        jnp.full((head_count, length), -1e30, jnp.float32),
        jnp.zeros((head_count, length), jnp.float32),
        jnp.zeros((length, head_count, head_dim), jnp.float32),
    )
    running = initial
    key_piece, value_piece = in_one_piece((key_rows, value_rows), "sp", 0, 1)
    piece_len = key_piece.shape[0]
    shards = piece_len // length
    group_size = max(
        [
            count_try
            for count_try in range(1, shards + 1)
            if shards % count_try == 0 and count_try * length <= max(length, 512)
        ]
    )
    block_len = group_size * length
    blocks = piece_len // block_len
    key_blocks = key_piece.reshape(blocks, block_len, head_count, head_dim)
    value_blocks = value_piece.reshape(blocks, block_len, head_count, head_dim)
    gate_blocks = gates_all.reshape(blocks, block_len, head_count)
    block_starts = block_len * jnp.arange(blocks, dtype=jnp.int32)

    def one_block(running_state, packed):
        key_block, value_block, gate_block, block_start = packed

        def compute(state_in):
            highest, totals, weighted = state_in
            scores = (
                jnp.einsum(
                    "qhd,khd->hqk", query_heads, key_block, preferred_element_type=jnp.float32
                )
                * score_scale
            )
            scores = scores + query_gates[:, :, None] - gate_block.T[:, None, :]
            key_pos = block_start + jnp.arange(block_len, dtype=jnp.int32)
            allowed = (key_pos[None, :] <= query_pos[:, None])[None]
            masked = jnp.where(allowed, scores, -1e30)
            new_high = jnp.maximum(highest, jnp.max(masked, axis=2))
            weights = jnp.where(allowed, jnp.exp(masked - new_high[:, :, None]), 0.0)
            factor = jnp.exp(highest - new_high)
            totals = totals * factor + jnp.sum(weights, axis=2)
            weighted = weighted * factor.T[:, :, None] + jnp.einsum(
                "hqk,khd->qhd",
                weights.astype(jnp.bfloat16),
                value_block,
                preferred_element_type=jnp.float32,
            )
            return (new_high, totals, weighted)

        def keep_state(state_in):
            return state_in

        return (lax.cond(block_start < last_pos, compute, keep_state, running_state), None)

    running, unused = lax.scan(
        one_block, running, (key_blocks, value_blocks, gate_blocks, block_starts)
    )
    highest, totals, weighted = running
    return (weighted / totals.T[:, :, None]).reshape(length, row_width).astype(jnp.bfloat16)


def body(
    queries,
    key_rows,
    value_rows,
    log_forget,
    stream_in,
    out_weight,
    mix_gain,
    mix_bias,
    gate_weight,
    up_weight,
    down_weight,
    ffn_gain,
    ffn_bias,
):
    attended = attend(queries, key_rows, value_rows, log_forget)
    length = attended.shape[0]
    own_rows = length // lax.axis_size("tp")
    offset = lax.axis_index("tp") * own_rows
    summed = sum_at_owner(
        jnp.dot(attended, out_weight, preferred_element_type=jnp.float32).astype(jnp.bfloat16),
        "tp",
        0,
    )
    mix_out = lax.optimization_barrier(summed.astype(jnp.bfloat16)).astype(jnp.float32)
    stream_own = lax.dynamic_slice_in_dim(stream_in, offset, own_rows, 0)
    normed = layer_norm(
        ALPHA * stream_own.astype(jnp.float32) + mix_out, mix_gain, mix_bias
    ).astype(jnp.bfloat16)
    gathered = lax.all_gather(normed, "tp", axis=0, tiled=True)
    pieces = in_one_piece((gate_weight, up_weight), "sp", 0, 1)
    gate_part = jnp.dot(gathered, pieces[0], preferred_element_type=jnp.float32)
    up_part = jnp.dot(gathered, pieces[1], preferred_element_type=jnp.float32)
    hidden = (jax.nn.silu(gate_part) * up_part).astype(jnp.bfloat16)
    partial_terms = jnp.dot(
        hidden,
        lax.all_gather(down_weight, "sp", axis=1, tiled=True),
        preferred_element_type=jnp.float32,
    )
    lowered = lax.psum_scatter(
        partial_terms.astype(jnp.bfloat16), "tp", scatter_dimension=0, tiled=True
    ).astype(jnp.float32)
    lowered = lax.optimization_barrier(lowered.astype(jnp.bfloat16)).astype(jnp.float32)
    result = layer_norm(ALPHA * normed.astype(jnp.float32) + lowered, ffn_gain, ffn_bias)
    return result.astype(jnp.bfloat16)


def solution(mesh):
    placed = (
        P("sp", "tp"),
        P("sp", "tp"),
        P("sp", "tp"),
        P("sp", "tp"),
        P("sp", None),
        P("tp", None),
        P(),
        P(),
        P("sp", "tp"),
        P("sp", "tp"),
        P("tp", "sp"),
        P(),
        P(),
    )
    return jax.shard_map(
        body, mesh=mesh, in_specs=placed, out_specs=P(("sp", "tp"), None), check_vma=False
    )
```

profile of v0, /device:TPU:0, one launch (start us, length us, event | category | flops | bytes accessed | tf_op | source)
XLA Modules:
  0.0 604.3 jit_solution(4880820120093457124)
XLA Ops:
  6.5 0.0 copy-start
  6.5 0.0 all-gather.5.cloned.1.call-start
  6.5 2.2 pad_maximum_fusion
  8.7 0.0 all-gather.5.cloned.1.call-update
  8.8 0.0 all-gather.9.cloned.1.call-start
  8.8 1.8 pad_maximum_fusion.1
  10.6 0.0 all-gather.9.cloned.1.call-update
  10.6 1.4 broadcast_in_dim.56
  12.0 8.2 %all-to-all-start = ((f32[16,768,4]{1,2,0:T(4,128)}), f32[16,768,4]{1,2,0:T(4,128)S(1)}, u32[]{:S(2)}, u32[]{:S(2)}) async-start(f32[16,768,4]{1,2,0:T(4,128)} %broadcast_in_dim.56), calls=%async_computation | async-start | bytes 393216 | tf_op jit(solution)/shard_map/all_to_all | solution.py:18
  20.2 1.2 copy.18
  21.4 80.5 %all-gather.5.cloned.1.call-done = bf16[12288,512]{1,0:T(8,128)(2,1)} async-done(((bf16[768,512]{1,0:T(8,128)(2,1)}), bf16[12288,512]{1,0:T(8,128)(2,1)}) %all-gather.5.cloned.1.call-update) | async-done | bytes 12582928 | tf_op jit(solution)/shard_map/all_gather | solution.py:31
  101.9 10.1 %fusion.36 = (bf16[12288,256]{1,0:T(8,128)(2,1)}, bf16[12288,256]{1,0:T(8,128)(2,1)}) fusion(bf16[12288,512]{1,0:T(8,128)(2,1)} %all-gather.5.cloned.1.call-done), kind=kLoop, calls=%fused_computation.51 | loop fusion | bytes 25165824 | tf_op jit(solution)/shard_map/split | solution.py:31
  112.0 18.8 %reshape.82 = bf16[16,768,4,64]{3,2,1,0:T(4,128)(2,1)} reshape(bf16[12288,256]{1,0:T(8,128)(2,1)} %get-tuple-element.249) | data formatting | bytes 12582912 | tf_op jit(solution)/shard_map/reshape | solution.py:80
  130.8 18.1 %copy.20 = bf16[16,768,4,64]{1,3,2,0:T(8,128)(2,1)} copy(bf16[16,768,4,64]{3,2,1,0:T(4,128)(2,1)} %reshape.82) | data formatting | bytes 12582912
  148.9 18.8 %reshape.83 = bf16[16,768,4,64]{3,2,1,0:T(4,128)(2,1)} reshape(bf16[12288,256]{1,0:T(8,128)(2,1)} %get-tuple-element.248) | data formatting | bytes 12582912 | tf_op jit(solution)/shard_map/reshape | solution.py:81
  167.6 18.1 %copy.21 = bf16[16,768,4,64]{1,3,2,0:T(8,128)(2,1)} copy(bf16[16,768,4,64]{3,2,1,0:T(4,128)(2,1)} %reshape.83) | data formatting | bytes 12582912
  185.7 0.0 all-to-all-done
  185.7 0.1 broadcast_in_dim.55
  185.8 33.5 %while.15 = (s32[]{:T(128)}, f32[4,768]{1,0:T(4,128)S(1)}, f32[4,768]{1,0:T(4,128)S(1)}, f32[768,4,64]{0,2,1:T(8,128)S(1)}, s32[16]{0:T(128)S(1)}, /*index=5*/s3...) while((s32[]{:T(128)}, f32[4,768]{1,0:T(4,128)S(1)}, ...), condition=%wide.region_5.6_spmd.clone, body=%wide.region_0.5_spmd.clone.sunk | while | flops 649800192 | bytes 33738040 | solution.py:117
  185.8 0.6 dynamic_slice.50
  187.1 13.1 %conditional.3 = ((f32[4,768]{1,0:T(4,128)S(1)}, f32[4,768]{1,0:T(4,128)S(1)}, f32[768,4,64]{0,2,1:T(8,128)S(1)})) conditional(s32[]{:T(128)} %convert_element_type.100, (f32[4,768]{1,0:T(4,128)S(1)}, f32[4,768]{1,0:T(4,128)S(1)}, f32[768,4,64]{0,2,1:T(8,128)S(1)}) %tuple.41, (s32[]{:T(128)}, s32[]{:T(128)}, bf16[16,768,4,64]{1,3,2,0:T(8,128)(2,1)}, ...), branch_computations={%region_1.1_spmd, %region_2.4_spmd} | conditional | flops 649800192 | bytes 33734700 | solution.py:115
  187.1 0.7 iota_add_fusion
  187.7 0.4 broadcast_compare_fusion
  188.2 3.9 fusion.4
  192.0 4.6 fusion.11
  196.6 3.5 fusion.3
  200.2 0.6 dynamic_slice.50
  201.4 0.6 dynamic_slice.50
  202.7 0.6 dynamic_slice.50
  204.0 0.6 dynamic_slice.50
  205.3 0.6 dynamic_slice.50
  206.5 0.6 dynamic_slice.50
  207.8 0.6 dynamic_slice.50
  209.1 0.6 dynamic_slice.50
  210.4 0.6 dynamic_slice.50
  211.7 0.6 dynamic_slice.50
  212.9 0.6 dynamic_slice.50
  214.2 0.6 dynamic_slice.50
  215.5 0.6 dynamic_slice.50
  216.8 0.6 dynamic_slice.50
  218.0 0.6 dynamic_slice.50
  219.3 0.1 divide_convert_fusion
  219.4 2.7 convolution_convert_fusion.1
  222.1 4.6 all-to-all-start.1
  226.7 0.2 all-gather.7.cloned.1.call-start
  226.9 38.2 %all-to-all-done.1 = bf16[8,96,2048]{2,1,0:T(8,128)(2,1)} async-done(((bf16[8,96,2048]{2,1,0:T(8,128)(2,1)}), bf16[8,96,2048]{2,1,0:T(8,128)(2,1)}, u32[]{:S(2)}, u32[]{:S(2)}) %all-to-all-start.1) | async-done | bytes 3145760 | tf_op jit(solution)/shard_map/all_to_all | solution.py:41
  265.1 2.5 reduce_sum.59
  267.6 1.2 fusion.33
  268.8 1.3 multiply_reduce_fusion.1
  270.2 2.0 add_convert_fusion.1
  272.2 0.0 all-gather.7.cloned.1.call-update
  272.2 0.0 all-gather.11.cloned.1.call-start
  272.2 0.5 all-gather.11.cloned.1.call-update
  272.8 0.0 reduce-scatter.2.cloned.1.call-start
  272.8 0.0 all-gather.9.cloned.1.call-done
  272.8 220.0 %all-gather.7.cloned.1.call-done = bf16[768,2048]{1,0:T(8,128)(2,1)} async-done(((bf16[96,2048]{1,0:T(8,128)(2,1)}), bf16[768,2048]{1,0:T(8,128)(2,1)}) %all-gather.7.cloned.1.call-update) | async-done | bytes 3145744 | tf_op jit(solution)/shard_map/all_gather | solution.py:153
  492.8 6.5 %fusion.27 = f32[768,704]{0,1:T(8,128)} fusion(bf16[768,2048]{1,0:T(8,128)(2,1)} %all-gather.7.cloned.1.call-done, bf16[2048,1408]{0,1:T(8,128)(2,1)} %all-gather.9.cloned.1.call-done), kind=kOutput, calls=%fused_computation.31 | convolution fusion | flops 2214592512 | bytes 8192000 | tf_op jit(solution)/shard_map/dot_general | solution.py:155
  499.3 46.2 %all-gather.11.cloned.1.call-done = bf16[704,2048]{1,0:T(8,128)(2,1)} async-done(((bf16[704,128]{1,0:T(8,128)(2,1)}), bf16[704,2048]{1,0:T(8,128)(2,1)}) %all-gather.11.cloned.1.call-update) | async-done | bytes 2883600 | tf_op jit(solution)/shard_map/all_gather | solution.py:160
  545.5 12.4 %convolution_convert_fusion = bf16[768,2048]{1,0:T(8,128)(2,1)} fusion(bf16[704,2048]{1,0:T(8,128)(2,1)} %all-gather.11.cloned.1.call-done, f32[768,704]{0,1:T(8,128)} %fusion.27, bf16[768,2048]{1,0:T(8,128)(2,1)} %all-gather.7.cloned.1.call-done, bf16[2048,1408]{0,1:T(8,128)(2,1)} %all-gather.9.cloned.1.call-done), kind=kOutput, calls=%fused_computation.27 | convolution fusion | flops 4434001920 | bytes 14221312 | tf_op jit(solution)/shard_map/dot_general | solution.py:158
  557.9 0.0 reduce-scatter.2.cloned.1.call-update
  557.9 35.3 %reduce-scatter.2.cloned.1.call-done = bf16[96,2048]{1,0:T(8,128)(2,1)} async-done(((bf16[768,2048]{1,0:T(8,128)(2,1)}), bf16[96,2048]{1,0:T(8,128)(2,1)}) %reduce-scatter.2.cloned.1.call-update) | async-done | bytes 393232 | tf_op jit(solution)/shard_map/reduce_scatter | solution.py:163
  593.2 1.2 fusion.34
  594.4 1.3 multiply_reduce_fusion
  595.7 2.0 add_convert_fusion
  (55 shorter events, 0.3 us)
Async XLA Ops:
  6.5 212.9 %copy-start = (bf16[256,2048]{1,0:T(8,128)(2,1)S(1)}, bf16[256,2048]{1,0:T(8,128)(2,1)}, u32[]{:S(2)}) copy-start(bf16[256,2048]{1,0:T(8,128)(2,1)} %param.22) | copy-start | bytes 3145732
  6.5 95.4 %all-gather.5.cloned.1.call-start = ((), (), s32[]{:S(2)}) async-start(), calls=%async_computation.3 | async-start | bytes 13369344 | tf_op jit(solution)/shard_map/all_gather | solution.py:31
  8.8 264.1 %all-gather.9.cloned.1.call-start = ((), (), s32[]{:S(2)}) async-start(), calls=%async_computation.5 | async-start | bytes 6127616 | tf_op jit(solution)/shard_map/all_gather | solution.py:31
  12.0 173.7 %all-to-all-start = ((f32[16,768,4]{1,2,0:T(4,128)}), f32[16,768,4]{1,2,0:T(4,128)S(1)}, u32[]{:S(2)}, u32[]{:S(2)}) async-start(f32[16,768,4]{1,2,0:T(4,128)} %broadcast_in_dim.56), calls=%async_computation | async-start | bytes 393216 | tf_op jit(solution)/shard_map/all_to_all | solution.py:18
  167.6 18.2 %copy-start.2 = (f32[768,4]{0,1:T(4,128)S(1)}, f32[768,4]{0,1:T(4,128)}, u32[]{:S(2)}) copy-start(f32[768,4]{0,1:T(4,128)} %param.20) | copy-start | bytes 36868
  222.1 48.0 %copy-start.3 = (f32[2048]{0:T(1024)S(1)}, f32[2048]{0:T(1024)}, u32[]{:S(2)}) copy-start(f32[2048]{0:T(1024)} %param.24) | copy-start | bytes 24580
  222.1 48.0 %copy-start.4 = (f32[2048]{0:T(1024)S(1)}, f32[2048]{0:T(1024)}, u32[]{:S(2)}) copy-start(f32[2048]{0:T(1024)} %param.23) | copy-start | bytes 24580
  222.1 43.0 %all-to-all-start.1 = ((bf16[8,96,2048]{2,1,0:T(8,128)(2,1)}), bf16[8,96,2048]{2,1,0:T(8,128)(2,1)}, u32[]{:S(2)}, u32[]{:S(2)}) async-start(bf16[8,96,2048]{2,1,0:T(8,128)(2,1)} %bitcast.45), calls=%async_computation.1 | async-start | bytes 6291456 | tf_op jit(solution)/shard_map/all_to_all | solution.py:41
  226.7 266.1 %all-gather.7.cloned.1.call-start = ((), (), s32[]{:S(2)}) async-start(), calls=%async_computation.4 | async-start | bytes 3538944 | tf_op jit(solution)/shard_map/all_gather | solution.py:153
  272.2 273.3 %all-gather.11.cloned.1.call-start = ((), (), s32[]{:S(2)}) async-start(), calls=%async_computation.6 | async-start | bytes 3063808 | tf_op jit(solution)/shard_map/all_gather | solution.py:160
  272.8 320.4 %reduce-scatter.2.cloned.1.call-start = ((), (), s32[]{:S(2)}) async-start(), calls=%async_computation.7 | async-start | bytes 3538944 | tf_op jit(solution)/shard_map/reduce_scatter | solution.py:163
  499.3 93.9 %copy-start.1 = (bf16[96,2048]{1,0:T(8,128)(2,1)S(1)}, bf16[96,2048]{1,0:T(8,128)(2,1)}, u32[]{:S(2)}) copy-start(bf16[96,2048]{1,0:T(8,128)(2,1)} %add_convert_fusion.1) | copy-start | bytes 1179652
  499.3 96.4 %copy-start.5 = (f32[2048]{0:T(1024)S(1)}, f32[2048]{0:T(1024)}, u32[]{:S(2)}) copy-start(f32[2048]{0:T(1024)} %param.29) | copy-start | bytes 24580
  499.3 96.4 %copy-start.6 = (f32[2048]{0:T(1024)S(1)}, f32[2048]{0:T(1024)}, u32[]{:S(2)}) copy-start(f32[2048]{0:T(1024)} %param.28) | copy-start | bytes 24580
Sparse Core Ops, SparseCore 0:
  9.5 92.3 all-gather.4
  104.0 64.0 all-gather.8
  272.3 220.4 all-gather.6
  494.8 50.6 all-gather.10
  558.0 35.0 reduce-scatter.1
where the time goes:
time: 608 us; the launch traced here: 604 us
  waiting for transfers between devices  421 us (69%)
  local copies, waits for them, and re-layouts  95.9 us (16%)
  matrix products  30.1 us (5%)
  other arithmetic  20.1 us (3%)
  between operations  13.3 us (2%)
  starting transfers between devices  13.1 us (2%)
  loops' own time  11.1 us (2%)
    all_gather x1, waiting for transfers between devices, body(): gathered = lax.all_gather(normed, 'tp', axis=0, tiled=True)  220 us
    all_gather x2, waiting for transfers between devices, in_one_piece(): lax.all_gather(both, axis, axis=dim, tiled=True)  80.5 us
    all_gather x1, waiting for transfers between devices, body(): lax.all_gather(down_weight, 'sp', axis=1, tiled=True)  46.2 us
    all_to_all x1, waiting for transfers between devices, sum_at_owner(): lax.all_to_all(pieces, axis, split_axis=0, concat_axis=0, tiled=True)  38.2 us
    unnamed x17, local copies, waits for them, and re-layouts  37.4 us
    reduce_scatter x1, waiting for transfers between devices, body(): lax.psum_scatter(partial_terms.astype(jnp.bfloat16), 'tp', scatter_dimens...  35.3 us
    reshape x1, local copies, waits for them, and re-layouts, attend(): key_blocks = key_piece.reshape(blocks, block_len, head_count, head_dim)  18.8 us
    reshape x1, local copies, waits for them, and re-layouts, attend(): value_blocks = value_piece.reshape(blocks, block_len, head_count, head_dim)  18.8 us
  transfers between devices with their start and end apart: 7, of which 5 were waited for; matrix products, arithmetic and copies ran while one was open for 21% of the time, Pallas kernels for 0%

commit v1 on v0

v1 whole, which is shorter than its diff:
```python
import functools

import jax
import jax.numpy as jnp
from jax import lax
from jax.experimental import pallas as pl
from jax.experimental.pallas import tpu as pltpu
from jax.sharding import PartitionSpec as P

ALPHA = 8.0**0.25
EPSILON = 1e-05
MESH = pl.DeviceIdType.MESH
LOG2E = 1.4426950408889634
NEG = -1e30
BL = 768
QW = 512
NT = 6
NB = 16
HD = 64
KVR = 144
VMEM = pl.BlockSpec(memory_space=pltpu.VMEM)
ANY = pl.BlockSpec(memory_space=pl.ANY)


def layer_norm(matrix, norm_gain, norm_shift):
    centred = matrix - jnp.mean(matrix, axis=-1, keepdims=True)
    spread = jnp.mean(centred * centred, axis=-1, keepdims=True)
    return centred * lax.rsqrt(spread + EPSILON) * norm_gain + norm_shift


def parts(x):
    hi = x.astype(jnp.bfloat16).astype(jnp.float32)
    rest = x - hi
    mid = rest.astype(jnp.bfloat16).astype(jnp.float32)
    return hi, mid, rest - mid


def head_of(sp):
    z, y = sp // 4, sp % 4
    return (z // 2) * 2 + y // 2


def member_of(sp):
    z, y = sp // 4, sp % 4
    return (z % 2) * 2 + y % 2


def place_of(head, member):
    z = (head // 2) * 2 + member // 2
    y = (head % 2) * 2 + member % 2
    return z * 4 + y


def chunk_of(t, member):
    return (t // 2) * 8 + (member if t % 2 == 0 else 7 - member)


def exchange_kernel(q_ref, k_ref, v_ref, g_ref, kvl, qt, ksrc, qsrc, ks, kr, qs, qr):
    me = lax.axis_index("sp")
    z, y = me // 4, me % 4
    barrier = pltpu.get_barrier_semaphore()
    for o in range(1, 16):
        to = ((z + o // 4) % 4) * 4 + (y + o % 4) % 4
        pl.semaphore_signal(barrier, inc=1, device_id={"sp": to}, device_id_type=MESH)
    kt = k_ref[...].T
    vt = v_ref[...].T
    qtt = q_ref[...].T
    gates = g_ref[...]
    row = lax.broadcasted_iota(jnp.int32, (16, BL), 0)
    for h in range(4):
        g = gates[h : h + 1]
        first = jnp.broadcast_to(g[:, 0:1], (1, BL))
        rows = [jnp.ones((1, BL), jnp.float32)]
        rows += parts((first - g) * LOG2E) + parts(first * (-LOG2E))
        extra = jnp.zeros((16, BL), jnp.float32)
        for n, r in enumerate(rows):
            extra = jnp.where(row == n, r, extra)
        ksrc[h, 0:64] = kt[64 * h : 64 * h + 64]
        ksrc[h, 64:80] = extra.astype(jnp.bfloat16)
        ksrc[h, 80:144] = vt[64 * h : 64 * h + 64]
        for i in range(3):
            qsrc[3 * h + i] = qtt[64 * h : 64 * h + 64, 256 * i : 256 * i + 256]
    pl.semaphore_wait(barrier, 15)
    own = pltpu.make_async_copy(ksrc.at[head_of(me)], kvl.at[me], kr.at[me])
    own.start()
    sends = []
    for o in range(1, 16):
        to = ((z + o // 4) % 4) * 4 + (y + o % 4) % 4
        copy = pltpu.make_async_remote_copy(
            src_ref=ksrc.at[head_of(to)],
            dst_ref=kvl.at[me],
            send_sem=ks.at[o],
            recv_sem=kr.at[me],
            device_id={"sp": to},
            device_id_type=MESH,
        )
        copy.start()
        sends.append(copy)
    qsends = []
    for h in range(4):
        for i in range(3):
            n = 3 * h + i
            sub = 3 * me + i
            c, u = sub // 2, sub % 2
            r = c % 8
            high = r // 4
            member = r + high * (7 - 2 * r)
            slot = 2 * ((c // 8) * 2 + high) + u
            to = place_of(h, member)
            copy = pltpu.make_async_remote_copy(
                src_ref=qsrc.at[n],
                dst_ref=qt.at[slot],
                send_sem=qs.at[n],
                recv_sem=qr.at[slot],
                device_id={"sp": to},
                device_id_type=MESH,
            )
            local = pltpu.make_async_copy(qsrc.at[n], qt.at[slot], qr.at[slot])

            @pl.when(to != me)
            def _():
                copy.start()

            @pl.when(to == me)
            def _():
                local.start()

            qsends.append((to, copy))
    for copy in sends:
        copy.wait_send()
    for to, copy in qsends:

        @pl.when(to != me)
        def _():
            copy.wait_send()

    for b in range(NB):
        pltpu.make_async_copy(ksrc.at[0], kvl.at[b], kr.at[b]).wait()
    for s in range(2 * NT):
        pltpu.make_async_copy(qsrc.at[0], qt.at[s], qr.at[s]).wait()


def exchange(q, k, v, gates):
    return pl.pallas_call(
        exchange_kernel,
        name="exchange",
        out_shape=(
            jax.ShapeDtypeStruct((NB, KVR, BL), jnp.bfloat16),
            jax.ShapeDtypeStruct((2 * NT, HD, 256), jnp.bfloat16),
        ),
        in_specs=[VMEM] * 4,
        out_specs=(ANY, ANY),
        scratch_shapes=[
            pltpu.VMEM((4, KVR, BL), jnp.bfloat16),
            pltpu.VMEM((12, HD, 256), jnp.bfloat16),
            pltpu.SemaphoreType.DMA((16,)),
            pltpu.SemaphoreType.DMA((16,)),
            pltpu.SemaphoreType.DMA((12,)),
            pltpu.SemaphoreType.DMA((12,)),
        ],
        compiler_params=pltpu.CompilerParams(collective_id=0, has_side_effects=True),
        cost_estimate=pl.CostEstimate(flops=50 * 10**9, bytes_accessed=8 * 10**6, transcendentals=0),
    )(q, k, v, gates)


def attention_kernel(mm_ref, kvl, qt, o_ref, X, R, S0, S1, mx0, mx1, M, A, base):
    mm = mm_ref[0]
    for b in range(NB):
        X[b * BL : (b + 1) * BL, :] = kvl[b, 0:128, :].T
        gate_rows = kvl[b, 64:80, 0:128].astype(jnp.float32)
        base[b] = jnp.broadcast_to(gate_rows[4:5] + gate_rows[5:6] + gate_rows[6:7], (8, 128))
    row = lax.broadcasted_iota(jnp.int32, (64, QW), 0)
    ones = jnp.where((row >= 1) & (row < 4), 1.0, 0.0).astype(jnp.bfloat16)
    for t in range(NT):
        q = jnp.concatenate([qt[2 * t], qt[2 * t + 1]], axis=1).astype(jnp.float32)
        q = q * (LOG2E / 8)
        hi = q.astype(jnp.bfloat16)
        R[t, 0:64] = hi
        R[t, 64:128] = ones
        R[t, 128:192] = (q - hi.astype(jnp.float32)).astype(jnp.bfloat16)
        R[t, 192:256] = jnp.zeros((64, QW), jnp.bfloat16)
        M[t] = jnp.full((8, QW), NEG, jnp.float32)
        A[t] = jnp.zeros((80, QW), jnp.float32)

    def qk(b, t, S, mx):
        x = X[pl.ds(pl.multiple_of(b * BL, BL), BL), :]
        s = jnp.dot(
            jnp.concatenate([x, x], axis=1), R[t], preferred_element_type=jnp.float32
        )
        S[...] = s
        mx[...] = jnp.max(s.reshape(BL // 8, 8, QW), axis=0)

    def mask(b, c, S, mx):
        @pl.when(b * BL + BL > c * QW)
        def _():
            kp = b * BL + lax.broadcasted_iota(jnp.int32, (BL, QW), 0)
            qp = c * QW + lax.broadcasted_iota(jnp.int32, (BL, QW), 1)
            s = jnp.where(kp <= qp, S[...], NEG)
            S[...] = s
            mx[...] = jnp.max(s.reshape(BL // 8, 8, QW), axis=0)

    def pv(b, t, S, mx):
        m_old = M[t][0:1]
        bs = jnp.tile(base[b][0:1], (1, QW // 128))
        m_new = jnp.maximum(m_old, jnp.max(mx[...], axis=0, keepdims=True) + bs)
        p = jnp.exp2(S[...] - (m_new - bs)).astype(jnp.bfloat16)
        o = jnp.dot(kvl[b, 64:144], p, preferred_element_type=jnp.float32)
        A[t] = A[t] * jnp.exp2(m_old - m_new) + o
        M[t] = jnp.broadcast_to(m_new, (8, QW))

    for t in range(NT):
        c = chunk_of(t, mm)
        nb = lax.div(c * QW + QW - 1, BL) + 1
        qk(0, t, S0, mx0)
        mask(0, c, S0, mx0)

        def body(i, _):
            b = 2 * i
            nxt = jnp.minimum(b + 1, nb - 1)
            qk(nxt, t, S1, mx1)
            pv(b, t, S0, mx0)
            mask(nxt, c, S1, mx1)

            @pl.when(b + 1 < nb)
            def _():
                after = jnp.minimum(b + 2, nb - 1)
                qk(after, t, S0, mx0)
                pv(b + 1, t, S1, mx1)
                mask(after, c, S0, mx0)

            return 0

        lax.fori_loop(0, lax.div(nb + 1, 2), body, 0)
        a = A[t]
        o_ref[t] = (a[16:80] / a[0:1]).T.astype(jnp.bfloat16)


def attention(member, kvl, qt):
    return pl.pallas_call(
        attention_kernel,
        name="attention",
        out_shape=jax.ShapeDtypeStruct((NT, QW, HD), jnp.bfloat16),
        in_specs=[pl.BlockSpec(memory_space=pltpu.SMEM), VMEM, VMEM],
        out_specs=VMEM,
        scratch_shapes=[
            pltpu.VMEM((NB * BL, 128), jnp.bfloat16),
            pltpu.VMEM((NT, 256, QW), jnp.bfloat16),
            pltpu.VMEM((BL, QW), jnp.float32),
            pltpu.VMEM((BL, QW), jnp.float32),
            pltpu.VMEM((8, QW), jnp.float32),
            pltpu.VMEM((8, QW), jnp.float32),
            pltpu.VMEM((NT, 8, QW), jnp.float32),
            pltpu.VMEM((NT, 80, QW), jnp.float32),
            pltpu.VMEM((NB, 8, 128), jnp.float32),
        ],
        compiler_params=pltpu.CompilerParams(vmem_limit_bytes=48 * 2**20),
        cost_estimate=pl.CostEstimate(flops=40 * 10**9, bytes_accessed=8 * 10**6, transcendentals=0),
    )(member, kvl, qt)


def give_back_kernel(o_ref, att, ss, rs):
    me = lax.axis_index("sp")
    tp = lax.axis_index("tp")
    member = member_of(me)
    head = tp * 4 + head_of(me)
    for phase in range(2):
        for t in range(NT):
            c = chunk_of(t, member)
            for u in range(2):
                sub = 2 * c + u

                def one(w, _):
                    to_sp = sub // 3
                    piece = 8 * (sub % 3) + w
                    to_tp = piece // 3
                    spot = 32 * (piece % 3)
                    src = o_ref.at[t, pl.ds(pl.multiple_of(256 * u + 32 * w, 32), 32)]
                    dst = att.at[head, pl.ds(pl.multiple_of(spot, 32), 32)]
                    n = (2 * t + u) * 8 + w
                    copy = pltpu.make_async_remote_copy(
                        src_ref=src,
                        dst_ref=dst,
                        send_sem=ss.at[n],
                        recv_sem=rs,
                        device_id={"sp": to_sp, "tp": to_tp},
                        device_id_type=MESH,
                    )
                    mine = (to_sp == me) & (to_tp == tp)

                    @pl.when(jnp.logical_not(mine))
                    def _():
                        if phase == 0:
                            copy.start()
                        else:
                            copy.wait_send()

                    if phase == 0:

                        @pl.when(mine)
                        def _():
                            pltpu.make_async_copy(src, dst, rs).start()

                    return 0

                lax.fori_loop(0, 8, one, 0)
    pltpu.make_async_copy(att, att, rs).wait()


def give_back(o):
    return pl.pallas_call(
        give_back_kernel,
        name="give_back",
        out_shape=jax.ShapeDtypeStruct((32, 96, HD), jnp.bfloat16),
        in_specs=[VMEM],
        out_specs=ANY,
        scratch_shapes=[pltpu.SemaphoreType.DMA((96,)), pltpu.SemaphoreType.DMA],
        compiler_params=pltpu.CompilerParams(has_side_effects=True),
        cost_estimate=pl.CostEstimate(flops=10 * 10**9, bytes_accessed=10**6, transcendentals=0),
    )(o)


def body(
    queries,
    key_rows,
    value_rows,
    log_forget,
    stream_in,
    out_weight,
    mix_gain,
    mix_bias,
    gate_weight,
    up_weight,
    down_weight,
    ffn_gain,
    ffn_bias,
):
    member = member_of(lax.axis_index("sp")).astype(jnp.int32).reshape(1)
    kvl, qt = exchange(queries, key_rows, value_rows, log_forget.T)
    att = give_back(attention(member, kvl, qt))
    attended = att.transpose(1, 0, 2).reshape(96, 2048)
    offset = lax.axis_index("tp") * 96
    mixed = jnp.dot(
        attended,
        lax.all_gather(out_weight, "tp", axis=0, tiled=True),
        preferred_element_type=jnp.float32,
    )
    mix_out = lax.optimization_barrier(mixed.astype(jnp.bfloat16)).astype(jnp.float32)
    stream_own = lax.dynamic_slice_in_dim(stream_in, offset, 96, 0)
    normed = layer_norm(
        ALPHA * stream_own.astype(jnp.float32) + mix_out, mix_gain, mix_bias
    ).astype(jnp.bfloat16)
    gathered = lax.all_gather(normed, "tp", axis=0, tiled=True)
    both = lax.all_gather(
        jnp.concatenate([gate_weight, up_weight], axis=1), "sp", axis=0, tiled=True
    )
    gate_part = jnp.dot(gathered, both[:, :704], preferred_element_type=jnp.float32)
    up_part = jnp.dot(gathered, both[:, 704:], preferred_element_type=jnp.float32)
    hidden = (jax.nn.silu(gate_part) * up_part).astype(jnp.bfloat16)
    partial_terms = jnp.dot(
        hidden,
        lax.all_gather(down_weight, "sp", axis=1, tiled=True),
        preferred_element_type=jnp.float32,
    )
    lowered = lax.psum_scatter(
        partial_terms.astype(jnp.bfloat16), "tp", scatter_dimension=0, tiled=True
    ).astype(jnp.float32)
    lowered = lax.optimization_barrier(lowered.astype(jnp.bfloat16)).astype(jnp.float32)
    result = layer_norm(ALPHA * normed.astype(jnp.float32) + lowered, ffn_gain, ffn_bias)
    return result.astype(jnp.bfloat16)


def solution(mesh):
    placed = (
        P("sp", "tp"),
        P("sp", "tp"),
        P("sp", "tp"),
        P("sp", "tp"),
        P("sp", None),
        P("tp", None),
        P(),
        P(),
        P("sp", "tp"),
        P("sp", "tp"),
        P("tp", "sp"),
        P(),
        P(),
    )
    return jax.shard_map(
        body, mesh=mesh, in_specs=placed, out_specs=P(("sp", "tp"), None), check_vma=False
    )
```

time: 608 us -> 296 us (0.49)
  waiting for transfers between devices: 421 us -> 115 us
  Pallas kernels: 0 us -> 128 us
  local copies, waits for them, and re-layouts: 95.9 us -> 5.39 us
  starting transfers between devices: 13.1 us -> 0.16 us
  loops' own time: 11.1 us -> 0 us
  other arithmetic: 20.1 us -> 10.8 us
  matrix products: 30.1 us -> 23.1 us
    all_gather x1, waiting for transfers between devices: 220 us -> 32.4 us  [body(): gathered = lax.all_gather(normed, 'tp', axis=0, tiled=True)]
    pallas_call x0 -> x3, Pallas kernels: none -> 128 us  [the longest x1 71.4 us: exchange(): pl.pallas_call(exchange_kernel, name='exchange', out_shape=(jax.ShapeDtyp...]
    all_gather x2, waiting for transfers between devices: 80.5 us -> 0.04 us  [the longest x1 0.02 us: body(): lax.all_gather(out_weight, 'tp', axis=0, tiled=True)]
    all_to_all x2 -> x0, waiting for transfers between devices: 38.2 us -> none  [the longest x1 38.2 us: sum_at_owner(): lax.all_to_all(pieces, axis, split_axis=0, concat_axis=0, tiled=True)]
    reshape x2 -> x0, local copies, waits for them, and re-layouts: 37.6 us -> none  [the longest x1 18.8 us: attend(): key_blocks = key_piece.reshape(blocks, block_len, head_count, head_dim)]
    unnamed x17 -> x18, local copies, waits for them, and re-layouts: 37.4 us -> 3.94 us
    all_to_all x2 -> x0, starting transfers between devices: 12.7 us -> none  [the longest x1 8.16 us: from_everyone(): return lax.all_to_all(copies, axis, split_axis=0, concat_axis=0, tiled=True)]
    another operation x17 -> x0, loops' own time: 11.1 us -> none  [the longest x1 10.9 us: attend(): lax.scan(one_block, running, (key_blocks, value_blocks, gate_blocks, bloc...]
  transfers between devices with their start and end apart: 7 -> 5, of which waited for: 5 -> 3; matrix products, arithmetic and copies ran while one was open for 21% -> 7% of each run, Pallas kernels for 0% -> 43%
where the time goes in v1:
time: 296 us; the launch traced here: 295 us
  Pallas kernels  128 us (43%)
  waiting for transfers between devices  115 us (39%)
  matrix products  23.1 us (8%)
  between operations  13.4 us (5%)
  other arithmetic  10.8 us (4%)
  local copies, waits for them, and re-layouts  5.39 us (2%)
    pallas_call x1, Pallas kernels, exchange(): pl.pallas_call(exchange_kernel, name='exchange', out_shape=(jax.ShapeDtyp...  71.4 us
    all_gather x1, waiting for transfers between devices, body(): lax.all_gather(down_weight, 'sp', axis=1, tiled=True)  46 us
    reduce_scatter x1, waiting for transfers between devices, body(): lax.psum_scatter(partial_terms.astype(jnp.bfloat16), 'tp', scatter_dimens...  35.3 us
    all_gather x1, waiting for transfers between devices, body(): gathered = lax.all_gather(normed, 'tp', axis=0, tiled=True)  32.4 us
    pallas_call x1, Pallas kernels, attention(): pl.pallas_call(attention_kernel, name='attention', out_shape=jax.ShapeDty...  31.5 us
    pallas_call x1, Pallas kernels, give_back(): pl.pallas_call(give_back_kernel, name='give_back', out_shape=jax.ShapeDty...  24.6 us
    dot_general x1, matrix products, body(): jnp.dot(hidden, lax.all_gather(down_weight, 'sp', axis=1, tiled=True), pr...  11.5 us
    dot_general x1, matrix products, body(): jnp.dot(gathered, both[:, :704], preferred_element_type=jnp.float32)  6.72 us
  transfers between devices with their start and end apart: 5, of which 3 were waited for; matrix products, arithmetic and copies ran while one was open for 7% of the time, Pallas kernels for 43%

profile of v1, /device:TPU:0, one launch (start us, length us, event | category | flops | bytes accessed | tf_op | source)
XLA Modules:
  0.0 295.4 jit_solution(6690391848794867049)
XLA Ops:
  6.5 0.0 all-gather.5.cloned.1.call-start
  6.5 0.7 all-gather.5.cloned.1.call-update
  7.3 0.0 all-gather.9.cloned.1.call-start
  7.3 1.8 pad_maximum_fusion
  9.1 0.0 all-gather.9.cloned.1.call-update
  9.1 0.0 all-gather.7.cloned.1.call-start
  9.2 71.4 %exchange.1 = (bf16[16,144,768]{2,1,0:T(8,128)(2,1)}, bf16[12,64,256]{2,1,0:T(8,128)(2,1)}) custom-call(bf16[768,256]{1,0:T(8,128)(2,1)} %q_ref.1, bf16[768,256]{1,0:T(8,128)(2,1)} %k_ref.1, bf16[768,256]{1,0:T(8,128)(2,1)} %v_ref.1, f32[4,768]{1,0:T(4,128)} %bitcast.11), custom_call_target="tpu_custom_call" | custom-call | flops 49999998976 | bytes 8000000 | tf_op jit(solution)/shard_map/exchange/pallas_call | solution.py:144
  80.7 0.0 copy-start.1
  80.7 2.0 copy-done.1
  82.7 0.0 copy-start.2
  82.7 1.0 copy-done.2
  83.7 31.5 %attention.1.o_ref = bf16[6,512,64]{2,1,0:T(8,128)(2,1)S(1)} custom-call(s32[1]{0:T(128)} %bitcast.mm_ref, bf16[16,144,768]{2,1,0:T(8,128)(2,1)S(1)} %copy-done.1, bf16[12,64,256]{2,1,0:T(8,128)(2,1)S(1)} %copy-done.2), custom_call_target="tpu_custom_call" | custom-call | flops 40000000000 | bytes 8000000 | tf_op jit(solution)/shard_map/attention/pallas_call | solution.py:239
  115.2 0.0 copy-start
  115.2 0.9 copy-done
  116.1 24.6 %give_back.1 = bf16[32,96,64]{2,1,0:T(8,128)(2,1)} custom-call(bf16[6,512,64]{2,1,0:T(8,128)(2,1)} %copy-done), custom_call_target="tpu_custom_call" | custom-call | flops 10000000000 | bytes 1000000 | tf_op jit(solution)/shard_map/give_back/pallas_call | solution.py:310
  140.8 1.5 copy.14
  142.2 0.0 all-gather.5.cloned.1.call-done
  142.3 0.0 copy-start.4
  142.3 0.0 copy-start.5
  142.3 4.9 %convolution_convert_fusion.1 = bf16[96,2048]{1,0:T(8,128)(2,1)S(1)} fusion(bf16[96,2048]{0,1:T(8,128)(2,1)S(1)} %bitcast.9, bf16[2048,2048]{1,0:T(8,128)(2,1)} %all-gather.5.cloned.1.call-done), kind=kOutput, calls=%fused_computation.5 | convolution fusion | flops 805502976 | bytes 9175040 | tf_op jit(solution)/shard_map/dot_general | solution.py:342
  147.2 1.2 fusion.8
  148.4 1.3 multiply_reduce_fusion.1
  149.7 0.0 copy-done.4
  149.7 0.0 copy-done.5
  149.7 2.0 add_convert_fusion.1
  151.7 0.0 all-gather.7.cloned.1.call-update
  151.8 0.0 all-gather.11.cloned.1.call-start
  151.8 0.5 all-gather.11.cloned.1.call-update
  152.3 0.0 reduce-scatter.2.cloned.1.call-start
  152.4 0.0 all-gather.9.cloned.1.call-done
  152.4 32.4 %all-gather.7.cloned.1.call-done = bf16[768,2048]{1,0:T(8,128)(2,1)} async-done(((bf16[96,2048]{1,0:T(8,128)(2,1)}), bf16[768,2048]{1,0:T(8,128)(2,1)}) %all-gather.7.cloned.1.call-update) | async-done | bytes 3145744 | tf_op jit(solution)/shard_map/all_gather | solution.py:352
  184.8 0.0 copy-start.8
  184.8 6.7 %fusion.2 = f32[768,704]{0,1:T(8,128)} fusion(bf16[768,2048]{1,0:T(8,128)(2,1)} %all-gather.7.cloned.1.call-done, bf16[2048,1408]{0,1:T(8,128)(2,1)} %all-gather.9.cloned.1.call-done), kind=kOutput, calls=%fused_computation.3 | convolution fusion | flops 2214592512 | bytes 8192000 | tf_op jit(solution)/shard_map/dot_general | solution.py:356
  191.6 46.0 %all-gather.11.cloned.1.call-done = bf16[704,2048]{1,0:T(8,128)(2,1)} async-done(((bf16[704,128]{1,0:T(8,128)(2,1)}), bf16[704,2048]{1,0:T(8,128)(2,1)}) %all-gather.11.cloned.1.call-update) | async-done | bytes 2883600 | tf_op jit(solution)/shard_map/all_gather | solution.py:361
  237.5 0.0 copy-done.8
  237.5 11.5 %convolution_convert_fusion = bf16[768,2048]{1,0:T(8,128)(2,1)} fusion(bf16[704,2048]{1,0:T(8,128)(2,1)} %all-gather.11.cloned.1.call-done, f32[768,704]{0,1:T(8,128)} %fusion.2, bf16[768,2048]{1,0:T(8,128)(2,1)S(1)} %copy-done.8, bf16[2048,1408]{0,1:T(8,128)(2,1)} %all-gather.9.cloned.1.call-done), kind=kOutput, calls=%fused_computation | convolution fusion | flops 4434001920 | bytes 14221312 | tf_op jit(solution)/shard_map/dot_general | solution.py:359
  249.0 0.0 copy-start.3
  249.0 0.0 copy-start.6
  249.0 0.0 copy-start.7
  249.0 0.0 reduce-scatter.2.cloned.1.call-update
  249.1 35.3 %reduce-scatter.2.cloned.1.call-done = bf16[96,2048]{1,0:T(8,128)(2,1)} async-done(((bf16[768,2048]{1,0:T(8,128)(2,1)}), bf16[96,2048]{1,0:T(8,128)(2,1)}) %reduce-scatter.2.cloned.1.call-update) | async-done | bytes 393232 | tf_op jit(solution)/shard_map/reduce_scatter | solution.py:364
  284.3 0.0 copy-done.3
  284.3 1.2 fusion.9
  285.6 1.3 multiply_reduce_fusion
  286.8 0.0 copy-done.6
  286.9 0.0 copy-done.7
  286.9 2.0 add_convert_fusion
  (4 shorter events, 0.0 us)
Async XLA Ops:
  6.5 135.7 %all-gather.5.cloned.1.call-start = ((), (), s32[]{:S(2)}) async-start(), calls=%async_computation.1 | async-start | bytes 9437184 | tf_op jit(solution)/shard_map/all_gather | solution.py:344
  7.3 145.1 %all-gather.9.cloned.1.call-start = ((), (), s32[]{:S(2)}) async-start(), calls=%async_computation.3 | async-start | bytes 6127616 | tf_op jit(solution)/shard_map/all_gather | solution.py:353
  9.1 175.7 %all-gather.7.cloned.1.call-start = ((), (), s32[]{:S(2)}) async-start(), calls=%async_computation.2 | async-start | bytes 3538944 | tf_op jit(solution)/shard_map/all_gather | solution.py:352
  80.7 2.0 copy-start.1
  82.7 1.0 copy-start.2
  115.2 0.9 copy-start
  142.3 7.5 %copy-start.4 = (f32[2048]{0:T(1024)S(1)}, f32[2048]{0:T(1024)}, u32[]{:S(2)}) copy-start(f32[2048]{0:T(1024)} %param.20) | copy-start | bytes 24580
  142.3 7.5 %copy-start.5 = (f32[2048]{0:T(1024)S(1)}, f32[2048]{0:T(1024)}, u32[]{:S(2)}) copy-start(f32[2048]{0:T(1024)} %param.19) | copy-start | bytes 24580
  151.8 85.8 %all-gather.11.cloned.1.call-start = ((), (), s32[]{:S(2)}) async-start(), calls=%async_computation.4 | async-start | bytes 3063808 | tf_op jit(solution)/shard_map/all_gather | solution.py:361
  152.3 132.0 %reduce-scatter.2.cloned.1.call-start = ((), (), s32[]{:S(2)}) async-start(), calls=%async_computation.5 | async-start | bytes 3538944 | tf_op jit(solution)/shard_map/reduce_scatter | solution.py:364
  184.8 52.7 %copy-start.8 = (bf16[768,2048]{1,0:T(8,128)(2,1)S(1)}, bf16[768,2048]{1,0:T(8,128)(2,1)}, u32[]{:S(2)}) copy-start(bf16[768,2048]{1,0:T(8,128)(2,1)} %all-gather.7.cloned.1.call-done) | copy-start | bytes 9437188
  249.0 35.3 %copy-start.3 = (bf16[96,2048]{1,0:T(8,128)(2,1)S(1)}, bf16[96,2048]{1,0:T(8,128)(2,1)}, u32[]{:S(2)}) copy-start(bf16[96,2048]{1,0:T(8,128)(2,1)} %add_convert_fusion.1) | copy-start | bytes 1179652
  249.0 37.8 %copy-start.6 = (f32[2048]{0:T(1024)S(1)}, f32[2048]{0:T(1024)}, u32[]{:S(2)}) copy-start(f32[2048]{0:T(1024)} %param.25) | copy-start | bytes 24580
  249.0 37.8 %copy-start.7 = (f32[2048]{0:T(1024)S(1)}, f32[2048]{0:T(1024)}, u32[]{:S(2)}) copy-start(f32[2048]{0:T(1024)} %param.24) | copy-start | bytes 24580
Sparse Core Ops, SparseCore 0:
  9.0 52.0 all-gather.4
  63.3 64.6 all-gather.8
  151.9 32.9 all-gather.6
  186.8 50.6 all-gather.10
  249.2 35.0 reduce-scatter.1

commit v2 on v1

--- a/solution.py
+++ b/solution.py
@@ -55,13 +55,102 @@
     return (t // 2) * 8 + (member if t % 2 == 0 else 7 - member)
 
 
-def exchange_kernel(q_ref, k_ref, v_ref, g_ref, kvl, qt, ksrc, qsrc, ks, kr, qs, qr):
+def ring():
+    tp = lax.axis_index("tp")
+    x, core = tp // 2, tp % 2
+    right = ((x + 1) % 4) * 2 + core
+    left = ((x + 3) % 4) * 2 + core
+    far = ((x + 2) % 4) * 2 + core
+    return tp, x * 2 + 1 - core, right, left, far
+
+
+def greet_ring():
+    tp, sibling, right, left, far = ring()
+    barrier = pltpu.get_barrier_semaphore()
+    for peer in (sibling, right, left):
+        pl.semaphore_signal(barrier, inc=1, device_id={"tp": peer}, device_id_type=MESH)
+
+
+class RingGather:
+    def __init__(self, own, buf, send, recv):
+        self.own, self.buf, self.send, self.recv = own, buf, send, recv
+        self.rows = buf.shape[1]
+        self.half = self.rows // 2
+        self.count = 0
+        self.started = []
+
+    def push(self, src, slot, peer, half=None):
+        if half is None:
+            dst, sem = self.buf.at[slot], self.recv.at[slot, 0]
+        else:
+            cut = pl.ds(half * self.half, self.half)
+            dst, sem = self.buf.at[slot, cut], self.recv.at[slot, half]
+        copy = pltpu.make_async_remote_copy(
+            src_ref=src,
+            dst_ref=dst,
+            send_sem=self.send.at[self.count],
+            recv_sem=sem,
+            device_id={"tp": peer},
+            device_id_type=MESH,
+        )
+        copy.start()
+        self.count += 1
+        self.started.append(copy)
+
+    def part(self, slot, half):
+        return self.buf.at[slot, pl.ds(half * self.half, self.half)]
+
+    def arrive(self, slot, half=None):
+        if half is None:
+            ref, sem = self.buf.at[slot], self.recv.at[slot, 0]
+        else:
+            ref, sem = self.part(slot, half), self.recv.at[slot, half]
+        pltpu.make_async_copy(ref, ref, sem).wait()
+
+    def begin(self):
+        tp, sibling, right, left, far = ring()
+        self.push(self.own, tp, right)
+        self.push(self.own, tp, left)
+        self.push(self.own, tp, sibling)
+
+    def relay(self):
+        tp, sibling, right, left, far = ring()
+        self.arrive(left)
+        self.push(self.part(left, 0), left, right, 0)
+        self.push(self.buf.at[left], left, sibling)
+        self.arrive(right)
+        self.push(self.part(right, 1), right, left, 1)
+        self.push(self.buf.at[right], right, sibling)
+        for half in range(2):
+            self.arrive(far, half)
+            self.push(self.part(far, half), far, sibling, half)
+
+    def finish(self):
+        tp, sibling, right, left, far = ring()
+        x = tp // 2
+        other = 1 - tp % 2
+        self.arrive(sibling)
+        self.arrive(((x + 3) % 4) * 2 + other)
+        self.arrive(((x + 1) % 4) * 2 + other)
+        for half in range(2):
+            self.arrive(((x + 2) % 4) * 2 + other, half)
+        for copy in self.started:
+            copy.wait_send()
+
+
+def exchange_kernel(
+    q_ref, k_ref, v_ref, g_ref, w_ref, kvl, qt, wall, ksrc, qsrc, wsrc, ks, kr, qs, qr, ws, wr, wl
+):
     me = lax.axis_index("sp")
     z, y = me // 4, me % 4
     barrier = pltpu.get_barrier_semaphore()
     for o in range(1, 16):
         to = ((z + o // 4) % 4) * 4 + (y + o % 4) % 4
         pl.semaphore_signal(barrier, inc=1, device_id={"sp": to}, device_id_type=MESH)
+    greet_ring()
+    tp = lax.axis_index("tp")
+    load = pltpu.make_async_copy(w_ref, wsrc, wl.at[0])
+    load.start()
     kt = k_ref[...].T
     vt = v_ref[...].T
     qtt = q_ref[...].T
@@ -80,7 +169,8 @@
         ksrc[h, 80:144] = vt[64 * h : 64 * h + 64]
         for i in range(3):
             qsrc[3 * h + i] = qtt[64 * h : 64 * h + 64, 256 * i : 256 * i + 256]
-    pl.semaphore_wait(barrier, 15)
+    load.wait()
+    pl.semaphore_wait(barrier, 18)
     own = pltpu.make_async_copy(ksrc.at[head_of(me)], kvl.at[me], kr.at[me])
     own.start()
     sends = []
@@ -126,6 +216,13 @@
                 local.start()
 
             qsends.append((to, copy))
+    keep = pltpu.make_async_copy(wsrc, wall.at[tp], wl.at[1])
+    keep.start()
+    gather = RingGather(wsrc, wall, ws, wr)
+    gather.begin()
+    gather.relay()
+    gather.finish()
+    keep.wait()
     for copy in sends:
         copy.wait_send()
     for to, copy in qsends:
@@ -140,27 +237,32 @@
         pltpu.make_async_copy(qsrc.at[0], qt.at[s], qr.at[s]).wait()
 
 
-def exchange(q, k, v, gates):
+def exchange(q, k, v, gates, w):
     return pl.pallas_call(
         exchange_kernel,
         name="exchange",
         out_shape=(
             jax.ShapeDtypeStruct((NB, KVR, BL), jnp.bfloat16),
             jax.ShapeDtypeStruct((2 * NT, HD, 256), jnp.bfloat16),
+            jax.ShapeDtypeStruct((8, 256, 2048), jnp.bfloat16),
         ),
-        in_specs=[VMEM] * 4,
-        out_specs=(ANY, ANY),
+        in_specs=[VMEM] * 4 + [ANY],
+        out_specs=(ANY, ANY, ANY),
         scratch_shapes=[
             pltpu.VMEM((4, KVR, BL), jnp.bfloat16),
             pltpu.VMEM((12, HD, 256), jnp.bfloat16),
+            pltpu.VMEM((256, 2048), jnp.bfloat16),
             pltpu.SemaphoreType.DMA((16,)),
             pltpu.SemaphoreType.DMA((16,)),
             pltpu.SemaphoreType.DMA((12,)),
             pltpu.SemaphoreType.DMA((12,)),
+            pltpu.SemaphoreType.DMA((9,)),
+            pltpu.SemaphoreType.DMA((8, 2)),
+            pltpu.SemaphoreType.DMA((2,)),
         ],
         compiler_params=pltpu.CompilerParams(collective_id=0, has_side_effects=True),
         cost_estimate=pl.CostEstimate(flops=50 * 10**9, bytes_accessed=8 * 10**6, transcendentals=0),
-    )(q, k, v, gates)
+    )(q, k, v, gates, w)
 
 
 def attention_kernel(mm_ref, kvl, qt, o_ref, X, R, S0, S1, mx0, mx1, M, A, base):
@@ -319,6 +421,178 @@
     )(o)
 
 
+def mix_kernel(att, w_ref, stream, gain, bias, out, lhs, wbuf, res, ws, rs, send, recv):
+    tp = lax.axis_index("tp")
+    greet_ring()
+    loads = [pltpu.make_async_copy(w_ref.at[j], wbuf.at[j], ws.at[j]) for j in range(8)]
+    for load in loads:
+        load.start()
+    own = pltpu.make_async_copy(
+        stream.at[pl.ds(pl.multiple_of(tp * 96, 96), 96)], res, rs
+    )
+    own.start()
+    for h in range(32):
+        lhs[:, HD * h : HD * h + HD] = att[h]
+    total = None
+    for j in range(8):
+        loads[j].wait()
+        term = jnp.dot(
+            lhs[:, 256 * j : 256 * j + 256], wbuf[j], preferred_element_type=jnp.float32
+        )
+        total = term if total is None else total + term
+    own.wait()
+    mixed = total.astype(jnp.bfloat16).astype(jnp.float32)
+    p = ALPHA * res[...].astype(jnp.float32) + mixed
+    out[tp] = layer_norm(p, gain[...], bias[...]).astype(jnp.bfloat16)
+    pl.semaphore_wait(pltpu.get_barrier_semaphore(), 3)
+    gather = RingGather(out.at[tp], out, send, recv)
+    gather.begin()
+    gather.relay()
+    gather.finish()
+
+
+def mix(att, w, stream, gain, bias):
+    return pl.pallas_call(
+        mix_kernel,
+        name="mix",
+        out_shape=jax.ShapeDtypeStruct((8, 96, 2048), jnp.bfloat16),
+        in_specs=[VMEM, ANY, ANY, VMEM, VMEM],
+        out_specs=VMEM,
+        scratch_shapes=[
+            pltpu.VMEM((96, 2048), jnp.bfloat16),
+            pltpu.VMEM((8, 256, 2048), jnp.bfloat16),
+            pltpu.VMEM((96, 2048), jnp.bfloat16),
+            pltpu.SemaphoreType.DMA((8,)),
+            pltpu.SemaphoreType.DMA,
+            pltpu.SemaphoreType.DMA((9,)),
+            pltpu.SemaphoreType.DMA((8, 2)),
+        ],
+        compiler_params=pltpu.CompilerParams(collective_id=1, has_side_effects=True),
+        cost_estimate=pl.CostEstimate(flops=20 * 10**9, bytes_accessed=10**7, transcendentals=0),
+    )(att, w, stream, gain, bias)
+
+
+def ffn_kernel(
+    rows, both, down, gain, bias, out, wgu, wd, hid, pb, sib, z, rel, inn, wl, ss, sr, zs, zr
+):
+    tp = lax.axis_index("tp")
+    x, core = tp // 2, tp % 2
+    _, sibling, right, left, far = ring()
+    greet_ring()
+    load_gu = pltpu.make_async_copy(both, wgu, wl.at[0])
+    load_gu.start()
+    load_d = pltpu.make_async_copy(down, wd, wl.at[1])
+    load_d.start()
+    load_gu.wait()
+
+    def up(i, _):
+        r = rows[pl.ds(pl.multiple_of(i * 384, 384), 384), :]
+        gate = jnp.dot(r, wgu[:, :704], preferred_element_type=jnp.float32)
+        upper = jnp.dot(r, wgu[:, 704:], preferred_element_type=jnp.float32)
+        hid[pl.ds(pl.multiple_of(i * 384, 384), 384), :] = (
+            gate / (1.0 + jnp.exp(-gate)) * upper
+        ).astype(jnp.bfloat16)
+        return 0
+
+    lax.fori_loop(0, 2, up, 0)
+    load_d.wait()
+    pl.semaphore_wait(pltpu.get_barrier_semaphore(), 3)
+    chips = [(x + 2) % 4, (x + 1) % 4, (x + 3) % 4, x]
+
+    def to_sibling(n):
+        return pltpu.make_async_remote_copy(
+            src_ref=pb.at[n, 1 - core],
+            dst_ref=sib.at[n],
+            send_sem=ss.at[n],
+            recv_sem=sr.at[n],
+            device_id={"tp": sibling},
+            device_id_type=MESH,
+        )
+
+    def send(n, src, dst, peer):
+        return pltpu.make_async_remote_copy(
+            src_ref=src,
+            dst_ref=dst,
+            send_sem=zs.at[n],
+            recv_sem=zr.at[n],
+            device_id={"tp": peer},
+            device_id_type=MESH,
+        )
+
+    hops = [
+        send(0, z.at[0, pl.ds(0, 48)], rel.at[0], right),
+        send(1, z.at[0, pl.ds(48, 48)], rel.at[1], left),
+        send(2, z.at[1], inn.at[0], right),
+        send(3, z.at[2], inn.at[1], left),
+    ]
+
+    def product(n):
+        h = hid[pl.ds(pl.multiple_of(chips[n] * 192, 192), 192), :]
+        s = jnp.dot(h, wd[...], preferred_element_type=jnp.float32).astype(jnp.bfloat16)
+        pb[n, 0] = s[:96]
+        pb[n, 1] = s[96:]
+        to_sibling(n).start()
+
+    def pair(n):
+        to_sibling(n).wait_recv()
+        return pb[n, core].astype(jnp.float32) + sib[n].astype(jnp.float32)
+
+    product(0)
+    product(1)
+    z[0] = pair(0).astype(jnp.bfloat16)
+    hops[0].start()
+    hops[1].start()
+    product(2)
+    s = pair(1)
+    hops[0].wait_recv()
+    z[1, 0:48] = (s[:48] + rel[0].astype(jnp.float32)).astype(jnp.bfloat16)
+    z[1, 48:96] = s[48:].astype(jnp.bfloat16)
+    hops[2].start()
+    product(3)
+    s = pair(2)
+    hops[1].wait_recv()
+    z[2, 0:48] = s[:48].astype(jnp.bfloat16)
+    z[2, 48:96] = (s[48:] + rel[1].astype(jnp.float32)).astype(jnp.bfloat16)
+    hops[3].start()
+    s = pair(3)
+    hops[2].wait_recv()
+    hops[3].wait_recv()
+    s = s + inn[0].astype(jnp.float32) + inn[1].astype(jnp.float32)
+    lowered = s.astype(jnp.bfloat16).astype(jnp.float32)
+    normed = rows[pl.ds(pl.multiple_of(tp * 96, 96), 96), :].astype(jnp.float32)
+    out[...] = layer_norm(ALPHA * normed + lowered, gain[...], bias[...]).astype(jnp.bfloat16)
+    for n in range(4):
+        to_sibling(n).wait_send()
+        hops[n].wait_send()
+
+
+def ffn(rows, both, down, gain, bias):
+    return pl.pallas_call(
+        ffn_kernel,
+        name="ffn",
+        out_shape=jax.ShapeDtypeStruct((96, 2048), jnp.bfloat16),
+        in_specs=[VMEM, ANY, ANY, VMEM, VMEM],
+        out_specs=VMEM,
+        scratch_shapes=[
+            pltpu.VMEM((2048, 1408), jnp.bfloat16),
+            pltpu.VMEM((704, 2048), jnp.bfloat16),
+            pltpu.VMEM((768, 704), jnp.bfloat16),
+            pltpu.VMEM((4, 2, 96, 2048), jnp.bfloat16),
+            pltpu.VMEM((4, 96, 2048), jnp.bfloat16),
+            pltpu.VMEM((3, 96, 2048), jnp.bfloat16),
+            pltpu.VMEM((2, 48, 2048), jnp.bfloat16),
+            pltpu.VMEM((2, 96, 2048), jnp.bfloat16),
+            pltpu.SemaphoreType.DMA((2,)),
+            pltpu.SemaphoreType.DMA((4,)),
+            pltpu.SemaphoreType.DMA((4,)),
+            pltpu.SemaphoreType.DMA((4,)),
+            pltpu.SemaphoreType.DMA((4,)),
+        ],
+        compiler_params=pltpu.CompilerParams(collective_id=2, has_side_effects=True),
+        cost_estimate=pl.CostEstimate(flops=20 * 10**9, bytes_accessed=10**7, transcendentals=0),
+    )(rows, both, down, gain, bias)
+
+
 def body(
     queries,
     key_rows,
@@ -335,38 +609,14 @@
     ffn_bias,
 ):
     member = member_of(lax.axis_index("sp")).astype(jnp.int32).reshape(1)
-    kvl, qt = exchange(queries, key_rows, value_rows, log_forget.T)
+    kvl, qt, wall = exchange(queries, key_rows, value_rows, log_forget.T, out_weight)
     att = give_back(attention(member, kvl, qt))
-    attended = att.transpose(1, 0, 2).reshape(96, 2048)
-    offset = lax.axis_index("tp") * 96
-    mixed = jnp.dot(
-        attended,
-        lax.all_gather(out_weight, "tp", axis=0, tiled=True),
-        preferred_element_type=jnp.float32,
-    )
-    mix_out = lax.optimization_barrier(mixed.astype(jnp.bfloat16)).astype(jnp.float32)
-    stream_own = lax.dynamic_slice_in_dim(stream_in, offset, 96, 0)
-    normed = layer_norm(
-        ALPHA * stream_own.astype(jnp.float32) + mix_out, mix_gain, mix_bias
-    ).astype(jnp.bfloat16)
-    gathered = lax.all_gather(normed, "tp", axis=0, tiled=True)
+    normed = mix(att, wall, stream_in, mix_gain[None], mix_bias[None])
     both = lax.all_gather(
         jnp.concatenate([gate_weight, up_weight], axis=1), "sp", axis=0, tiled=True
     )
-    gate_part = jnp.dot(gathered, both[:, :704], preferred_element_type=jnp.float32)
-    up_part = jnp.dot(gathered, both[:, 704:], preferred_element_type=jnp.float32)
-    hidden = (jax.nn.silu(gate_part) * up_part).astype(jnp.bfloat16)
-    partial_terms = jnp.dot(
-        hidden,
-        lax.all_gather(down_weight, "sp", axis=1, tiled=True),
-        preferred_element_type=jnp.float32,
-    )
-    lowered = lax.psum_scatter(
-        partial_terms.astype(jnp.bfloat16), "tp", scatter_dimension=0, tiled=True
-    ).astype(jnp.float32)
-    lowered = lax.optimization_barrier(lowered.astype(jnp.bfloat16)).astype(jnp.float32)
-    result = layer_norm(ALPHA * normed.astype(jnp.float32) + lowered, ffn_gain, ffn_bias)
-    return result.astype(jnp.bfloat16)
+    down = lax.all_gather(down_weight, "sp", axis=1, tiled=True)
+    return ffn(normed.reshape(768, 2048), both, down, ffn_gain[None], ffn_bias[None])
 
 
 def solution(mesh):

time: 296 us -> 221 us (0.75)
  waiting for transfers between devices: 115 us -> 10.7 us
  Pallas kernels: 128 us -> 187 us
  matrix products: 23.1 us -> 0 us
  other arithmetic: 10.8 us -> 0.86 us
    all_gather x3 -> x1, waiting for transfers between devices: 78.4 us -> 0.02 us  [body(): down = lax.all_gather(down_weight, 'sp', axis=1, tiled=True)]
    pallas_call x0 -> x2, Pallas kernels: none -> 59.8 us  [the longest x1 31.7 us: ffn(): pl.pallas_call(ffn_kernel, name='ffn', out_shape=jax.ShapeDtypeStruct((96...]
    reduce_scatter x1 -> x0, waiting for transfers between devices: 35.3 us -> none  [body(): lax.psum_scatter(partial_terms.astype(jnp.bfloat16), 'tp', scatter_dimens...]
    dot_general x3 -> x0, matrix products: 23.1 us -> none  [the longest x1 11.5 us: body(): jnp.dot(hidden, lax.all_gather(down_weight, 'sp', axis=1, tiled=True), pr...]
    all_gather x1, waiting for transfers between devices: 0.02 us -> 9.96 us  [body(): lax.all_gather(jnp.concatenate([gate_weight, up_weight], axis=1), 'sp', a...]
    reduce_sum x4 -> x0, other arithmetic: 5.01 us -> none  [the longest x2 2.56 us: layer_norm(): spread = jnp.mean(centred * centred, axis=-1, keepdims=True)]
    convert_element_type x2 -> x0, other arithmetic: 3.99 us -> none  [the longest x1 2 us: body(): normed = layer_norm(ALPHA * stream_own.astype(jnp.float32) + mix_out, mix...]
    unnamed x18 -> x9, local copies, waits for them, and re-layouts: 3.94 us -> 7.74 us
  transfers between devices with their start and end apart: 5 -> 2, of which waited for: 3 -> 1; matrix products, arithmetic and copies ran while one was open for 7% -> 1% of each run, Pallas kernels for 43% -> 71%
where the time goes in v2:
time: 221 us; the launch traced here: 220 us
  Pallas kernels  187 us (85%)
  between operations  13.5 us (6%)
  waiting for transfers between devices  10.7 us (5%)
  local copies, waits for them, and re-layouts  7.74 us (4%)
    pallas_call x1, Pallas kernels, exchange(): pl.pallas_call(exchange_kernel, name='exchange', out_shape=(jax.ShapeDtyp...  71.2 us
    pallas_call x1, Pallas kernels, attention(): pl.pallas_call(attention_kernel, name='attention', out_shape=jax.ShapeDty...  31.7 us
    pallas_call x1, Pallas kernels, ffn(): pl.pallas_call(ffn_kernel, name='ffn', out_shape=jax.ShapeDtypeStruct((96...  31.7 us
    pallas_call x1, Pallas kernels, mix(): pl.pallas_call(mix_kernel, name='mix', out_shape=jax.ShapeDtypeStruct((8,...  28.1 us
    pallas_call x1, Pallas kernels, give_back(): pl.pallas_call(give_back_kernel, name='give_back', out_shape=jax.ShapeDty...  24.7 us
    all_gather x1, waiting for transfers between devices, body(): lax.all_gather(jnp.concatenate([gate_weight, up_weight], axis=1), 'sp', a...  9.96 us
    unnamed x9, local copies, waits for them, and re-layouts  7.74 us
  transfers between devices with their start and end apart: 2, of which 1 were waited for; matrix products, arithmetic and copies ran while one was open for 1% of the time, Pallas kernels for 71%

profile of v2, /device:TPU:0, one launch (start us, length us, event | category | flops | bytes accessed | tf_op | source)
XLA Modules:
  0.0 220.2 jit_solution(8465263784570683167)
XLA Ops:
  6.5 0.0 all-gather.5.cloned.1.call-start
  6.5 0.7 all-gather.5.cloned.1.call-update
  7.3 0.0 all-gather.3.cloned.1.call-start
  7.3 1.1 copy.14
  8.4 1.1 copy.15
  9.4 0.9 pad_maximum_fusion
  10.3 0.0 all-gather.3.cloned.1.call-update
  10.4 71.2 %exchange.1 = (bf16[16,144,768]{2,1,0:T(8,128)(2,1)}, bf16[12,64,256]{2,1,0:T(8,128)(2,1)}, bf16[8,256,2048]{2,1,0:T(8,128)(2,1)}) custom-call(bf16[768,256]{1,0:T(8,128)(2,1)} %q_ref.1, bf16[768,256]{1,0:T(8,128)(2,1)} %k_ref.1, bf16[768,256]{1,0:T(8,128)(2,1)} %v_ref.1, f32[4,768]{1,0:T(4,128)} %bitcast.7, bf16[256,2048]{1,0:T(8,128)(2,1)} %w_ref.1), custom_call_target="tpu_custom_call" | custom-call | flops 49999998976 | bytes 8000000 | tf_op jit(solution)/shard_map/exchange/pallas_call | solution.py:241
  81.6 0.0 copy-start.1
  81.6 2.0 copy-done.1
  83.6 0.0 copy-start.2
  83.6 1.0 copy-done.2
  84.6 31.7 %attention.1.o_ref = bf16[6,512,64]{2,1,0:T(8,128)(2,1)S(1)} custom-call(s32[1]{0:T(128)} %bitcast.mm_ref, bf16[16,144,768]{2,1,0:T(8,128)(2,1)S(1)} %copy-done.1, bf16[12,64,256]{2,1,0:T(8,128)(2,1)S(1)} %copy-done.2), custom_call_target="tpu_custom_call" | custom-call | flops 40000000000 | bytes 8000000 | tf_op jit(solution)/shard_map/attention/pallas_call | solution.py:341
  116.3 0.0 copy-start
  116.3 0.9 copy-done
  117.1 24.7 %give_back.1.att = bf16[32,96,64]{2,1,0:T(8,128)(2,1)} custom-call(bf16[6,512,64]{2,1,0:T(8,128)(2,1)} %copy-done), custom_call_target="tpu_custom_call" | custom-call | flops 10000000000 | bytes 1000000 | tf_op jit(solution)/shard_map/give_back/pallas_call | solution.py:412
  141.8 28.1 %mix.1 = bf16[8,96,2048]{2,1,0:T(8,128)(2,1)} custom-call(bf16[32,96,64]{2,1,0:T(8,128)(2,1)} %give_back.1.att, bf16[8,256,2048]{2,1,0:T(8,128)(2,1)} %get-tuple-element.10.w_ref, bf16[768,2048]{1,0:T(8,128)(2,1)} %stream.1, f32[1,2048]{1,0:T(1,128)} %bitcast.8, f32[1,2048]{1,0:T(1,128)} %bitcast.9), custom_call_target="tpu_custom_call" | custom-call | flops 20000000000 | bytes 10000000 | tf_op jit(solution)/shard_map/mix/pallas_call | solution.py:455
  169.9 0.0 all-gather.5.cloned.1.call-done.down
  170.0 10.0 %all-gather.3.cloned.1.call-done.both = bf16[2048,1408]{1,0:T(8,128)(2,1)} async-done(((bf16[128,1408]{1,0:T(8,128)(2,1)}), bf16[2048,1408]{1,0:T(8,128)(2,1)}) %all-gather.3.cloned.1.call-update) | async-done | bytes 5767184 | tf_op jit(solution)/shard_map/all_gather | solution.py:615
  179.9 31.7 %ffn.1 = bf16[96,2048]{1,0:T(8,128)(2,1)} custom-call(bf16[768,2048]{1,0:T(8,128)(2,1)} %bitcast.12, bf16[2048,1408]{1,0:T(8,128)(2,1)} %all-gather.3.cloned.1.call-done.both, bf16[704,2048]{1,0:T(8,128)(2,1)} %all-gather.5.cloned.1.call-done.down, f32[1,2048]{1,0:T(1,128)} %bitcast.10, f32[1,2048]{1,0:T(1,128)} %bitcast.11), custom_call_target="tpu_custom_call" | custom-call | flops 20000000000 | bytes 10000000 | tf_op jit(solution)/shard_map/ffn/pallas_call | solution.py:570
  211.6 1.8 copy.17
Async XLA Ops:
  6.5 163.4 %all-gather.5.cloned.1.call-start = ((), (), s32[]{:S(2)}) async-start(), calls=%async_computation.1 | async-start | bytes 3063808 | tf_op jit(solution)/shard_map/all_gather | solution.py:618
  7.3 172.7 %all-gather.3.cloned.1.call-start = ((), (), s32[]{:S(2)}) async-start(), calls=%async_computation | async-start | bytes 6127616 | tf_op jit(solution)/shard_map/all_gather | solution.py:615
  81.6 2.0 copy-start.1
  83.6 1.0 copy-start.2
  116.3 0.9 copy-start
Sparse Core Ops, SparseCore 0:
  9.4 97.1 all-gather.4
  108.8 71.0 all-gather.2

commit v3 on v2

--- a/solution.py
+++ b/solution.py
@@ -13,6 +13,8 @@
 LOG2E = 1.4426950408889634
 NEG = -1e30
 BL = 768
+ORDER = tuple(range(1, 16))
+RELAY = (8, 9, 14)
 QW = 512
 NT = 6
 NB = 16
@@ -77,7 +79,6 @@
         self.rows = buf.shape[1]
         self.half = self.rows // 2
         self.count = 0
-        self.started = []
 
     def push(self, src, slot, peer, half=None):
         if half is None:
@@ -95,7 +96,6 @@
         )
         copy.start()
         self.count += 1
-        self.started.append(copy)
 
     def part(self, slot, half):
         return self.buf.at[slot, pl.ds(half * self.half, self.half)]
@@ -109,21 +109,30 @@
 
     def begin(self):
         tp, sibling, right, left, far = ring()
+        self.count = 0
         self.push(self.own, tp, right)
         self.push(self.own, tp, left)
         self.push(self.own, tp, sibling)
 
+    def stage(self, n):
+        tp, sibling, right, left, far = ring()
+        self.count = 3 + 2 * n
+        if n == 0:
+            self.arrive(left)
+            self.push(self.part(left, 0), left, right, 0)
+            self.push(self.buf.at[left], left, sibling)
+        elif n == 1:
+            self.arrive(right)
+            self.push(self.part(right, 1), right, left, 1)
+            self.push(self.buf.at[right], right, sibling)
+        else:
+            for half in range(2):
+                self.arrive(far, half)
+                self.push(self.part(far, half), far, sibling, half)
+
     def relay(self):
-        tp, sibling, right, left, far = ring()
-        self.arrive(left)
-        self.push(self.part(left, 0), left, right, 0)
-        self.push(self.buf.at[left], left, sibling)
-        self.arrive(right)
-        self.push(self.part(right, 1), right, left, 1)
-        self.push(self.buf.at[right], right, sibling)
-        for half in range(2):
-            self.arrive(far, half)
-            self.push(self.part(far, half), far, sibling, half)
+        for n in range(3):
+            self.stage(n)
 
     def finish(self):
         tp, sibling, right, left, far = ring()
@@ -134,21 +143,36 @@
         self.arrive(((x + 1) % 4) * 2 + other)
         for half in range(2):
             self.arrive(((x + 2) % 4) * 2 + other, half)
-        for copy in self.started:
-            copy.wait_send()
-
-
-def exchange_kernel(
-    q_ref, k_ref, v_ref, g_ref, w_ref, kvl, qt, wall, ksrc, qsrc, wsrc, ks, kr, qs, qr, ws, wr, wl
+        for n in range(9):
+            ref = self.own if n not in (3, 5, 7, 8) else self.part(0, 0)
+            pltpu.make_async_copy(ref, ref, self.send.at[n]).wait()
+
+
+def greet_all():
+    me = lax.axis_index("sp")
+    tp = lax.axis_index("tp")
+    barrier = pltpu.get_barrier_semaphore()
+
+    def one(i, _):
+        sp = (me + i // 8) % 16
+        to = (tp + i % 8) % 8
+        pl.semaphore_signal(
+            barrier, inc=1, device_id={"sp": sp, "tp": to}, device_id_type=MESH
+        )
+        return 0
+
+    lax.fori_loop(1, 128, one, 0)
+
+
+def attend_kernel(
+    q_ref, k_ref, v_ref, g_ref, w_ref, att, wall,
+    kvl, qt, ksrc, qsrc, wsrc, X, R, S0, S1, mx0, mx1, M, A, O,
+    ks, kr, qs, qr, ws, wr, wl, gs, gr,
 ):
     me = lax.axis_index("sp")
+    tp = lax.axis_index("tp")
     z, y = me // 4, me % 4
-    barrier = pltpu.get_barrier_semaphore()
-    for o in range(1, 16):
-        to = ((z + o // 4) % 4) * 4 + (y + o % 4) % 4
-        pl.semaphore_signal(barrier, inc=1, device_id={"sp": to}, device_id_type=MESH)
-    greet_ring()
-    tp = lax.axis_index("tp")
+    greet_all()
     load = pltpu.make_async_copy(w_ref, wsrc, wl.at[0])
     load.start()
     kt = k_ref[...].T
@@ -170,22 +194,7 @@
         for i in range(3):
             qsrc[3 * h + i] = qtt[64 * h : 64 * h + 64, 256 * i : 256 * i + 256]
     load.wait()
-    pl.semaphore_wait(barrier, 18)
-    own = pltpu.make_async_copy(ksrc.at[head_of(me)], kvl.at[me], kr.at[me])
-    own.start()
-    sends = []
-    for o in range(1, 16):
-        to = ((z + o // 4) % 4) * 4 + (y + o % 4) % 4
-        copy = pltpu.make_async_remote_copy(
-            src_ref=ksrc.at[head_of(to)],
-            dst_ref=kvl.at[me],
-            send_sem=ks.at[o],
-            recv_sem=kr.at[me],
-            device_id={"sp": to},
-            device_id_type=MESH,
-        )
-        copy.start()
-        sends.append(copy)
+    pl.semaphore_wait(pltpu.get_barrier_semaphore(), 127)
     qsends = []
     for h in range(4):
         for i in range(3):
@@ -216,64 +225,31 @@
                 local.start()
 
             qsends.append((to, copy))
+    sends = []
+    for o in ORDER:
+        to = ((z + o // 4) % 4) * 4 + (y + o % 4) % 4
+        copy = pltpu.make_async_remote_copy(
+            src_ref=ksrc.at[head_of(to)],
+            dst_ref=kvl.at[me],
+            send_sem=ks.at[o],
+            recv_sem=kr.at[me],
+            device_id={"sp": to},
+            device_id_type=MESH,
+        )
+        copy.start()
+        sends.append(copy)
+    own = pltpu.make_async_copy(ksrc.at[head_of(me)], kvl.at[me], kr.at[me])
+    own.start()
     keep = pltpu.make_async_copy(wsrc, wall.at[tp], wl.at[1])
     keep.start()
     gather = RingGather(wsrc, wall, ws, wr)
     gather.begin()
-    gather.relay()
-    gather.finish()
-    keep.wait()
-    for copy in sends:
-        copy.wait_send()
-    for to, copy in qsends:
-
-        @pl.when(to != me)
-        def _():
-            copy.wait_send()
-
-    for b in range(NB):
-        pltpu.make_async_copy(ksrc.at[0], kvl.at[b], kr.at[b]).wait()
-    for s in range(2 * NT):
-        pltpu.make_async_copy(qsrc.at[0], qt.at[s], qr.at[s]).wait()
-
-
-def exchange(q, k, v, gates, w):
-    return pl.pallas_call(
-        exchange_kernel,
-        name="exchange",
-        out_shape=(
-            jax.ShapeDtypeStruct((NB, KVR, BL), jnp.bfloat16),
-            jax.ShapeDtypeStruct((2 * NT, HD, 256), jnp.bfloat16),
-            jax.ShapeDtypeStruct((8, 256, 2048), jnp.bfloat16),
-        ),
-        in_specs=[VMEM] * 4 + [ANY],
-        out_specs=(ANY, ANY, ANY),
-        scratch_shapes=[
-            pltpu.VMEM((4, KVR, BL), jnp.bfloat16),
-            pltpu.VMEM((12, HD, 256), jnp.bfloat16),
-            pltpu.VMEM((256, 2048), jnp.bfloat16),
-            pltpu.SemaphoreType.DMA((16,)),
-            pltpu.SemaphoreType.DMA((16,)),
-            pltpu.SemaphoreType.DMA((12,)),
-            pltpu.SemaphoreType.DMA((12,)),
-            pltpu.SemaphoreType.DMA((9,)),
-            pltpu.SemaphoreType.DMA((8, 2)),
-            pltpu.SemaphoreType.DMA((2,)),
-        ],
-        compiler_params=pltpu.CompilerParams(collective_id=0, has_side_effects=True),
-        cost_estimate=pl.CostEstimate(flops=50 * 10**9, bytes_accessed=8 * 10**6, transcendentals=0),
-    )(q, k, v, gates, w)
-
-
-def attention_kernel(mm_ref, kvl, qt, o_ref, X, R, S0, S1, mx0, mx1, M, A, base):
-    mm = mm_ref[0]
-    for b in range(NB):
-        X[b * BL : (b + 1) * BL, :] = kvl[b, 0:128, :].T
-        gate_rows = kvl[b, 64:80, 0:128].astype(jnp.float32)
-        base[b] = jnp.broadcast_to(gate_rows[4:5] + gate_rows[5:6] + gate_rows[6:7], (8, 128))
+
     row = lax.broadcasted_iota(jnp.int32, (64, QW), 0)
     ones = jnp.where((row >= 1) & (row < 4), 1.0, 0.0).astype(jnp.bfloat16)
     for t in range(NT):
+        for u in range(2):
+            pltpu.make_async_copy(qsrc.at[0], qt.at[2 * t + u], qr.at[2 * t + u]).wait()
         q = jnp.concatenate([qt[2 * t], qt[2 * t + 1]], axis=1).astype(jnp.float32)
         q = q * (LOG2E / 8)
         hi = q.astype(jnp.bfloat16)
@@ -284,68 +260,159 @@
         M[t] = jnp.full((8, QW), NEG, jnp.float32)
         A[t] = jnp.zeros((80, QW), jnp.float32)
 
-    def qk(b, t, S, mx):
-        x = X[pl.ds(pl.multiple_of(b * BL, BL), BL), :]
+    mm = member_of(me)
+    S = (S0, S1)
+    mx = (mx0, mx1)
+
+    def qk(t, n):
+        x = X[...]
         s = jnp.dot(
             jnp.concatenate([x, x], axis=1), R[t], preferred_element_type=jnp.float32
         )
-        S[...] = s
-        mx[...] = jnp.max(s.reshape(BL // 8, 8, QW), axis=0)
-
-    def mask(b, c, S, mx):
+        S[n][...] = s
+        mx[n][...] = jnp.max(s.reshape(BL // 8, 8, QW), axis=0)
+
+    def mask(b, t, n):
+        c = chunk_of(t, mm)
+
         @pl.when(b * BL + BL > c * QW)
         def _():
             kp = b * BL + lax.broadcasted_iota(jnp.int32, (BL, QW), 0)
             qp = c * QW + lax.broadcasted_iota(jnp.int32, (BL, QW), 1)
-            s = jnp.where(kp <= qp, S[...], NEG)
-            S[...] = s
-            mx[...] = jnp.max(s.reshape(BL // 8, 8, QW), axis=0)
-
-    def pv(b, t, S, mx):
+            s = jnp.where(kp <= qp, S[n][...], NEG)
+            S[n][...] = s
+            mx[n][...] = jnp.max(s.reshape(BL // 8, 8, QW), axis=0)
+
+    def pv(b, t, n, bs):
         m_old = M[t][0:1]
-        bs = jnp.tile(base[b][0:1], (1, QW // 128))
-        m_new = jnp.maximum(m_old, jnp.max(mx[...], axis=0, keepdims=True) + bs)
-        p = jnp.exp2(S[...] - (m_new - bs)).astype(jnp.bfloat16)
+        m_new = jnp.maximum(m_old, jnp.max(mx[n][...], axis=0, keepdims=True) + bs)
+        p = jnp.exp2(S[n][...] - (m_new - bs)).astype(jnp.bfloat16)
         o = jnp.dot(kvl[b, 64:144], p, preferred_element_type=jnp.float32)
         A[t] = A[t] * jnp.exp2(m_old - m_new) + o
         M[t] = jnp.broadcast_to(m_new, (8, QW))
 
+    def block(i, _):
+        o = i
+        b = ((z + 4 - o // 4) % 4) * 4 + (y + 4 - o % 4) % 4
+        pltpu.make_async_copy(ksrc.at[0], kvl.at[b], kr.at[b]).wait()
+        X[...] = kvl[b, 0:128, :].T
+        g = kvl[b, 64:80, 0:128].astype(jnp.float32)
+        bs = jnp.tile(g[4:5] + g[5:6] + g[6:7], (1, QW // 128))
+
+        def live(t):
+            return chunk_of(t, mm) * QW + QW > b * BL
+
+        for t in range(NT):
+            first = live(t) if t == 0 else live(t) & jnp.logical_not(live(t - 1))
+
+            @pl.when(first)
+            def _():
+                qk(t, t % 2)
+                mask(b, t, t % 2)
+
+            @pl.when(live(t))
+            def _():
+                if t + 1 < NT:
+                    qk(t + 1, (t + 1) % 2)
+                pv(b, t, t % 2, bs)
+                if t + 1 < NT:
+                    mask(b, t + 1, (t + 1) % 2)
+
+        for stage in range(3):
+
+            @pl.when(i == RELAY[stage])
+            def _():
+                gather.stage(stage)
+
+        return 0
+
+    lax.fori_loop(0, 16, block, 0)
+
+    head = tp * 4 + head_of(me)
+
+    def piece(t, u, w):
+        sub = 2 * chunk_of(t, mm) + u
+        n = 8 * (sub % 3) + w
+        to_sp, to_tp, spot = sub // 3, n // 3, n % 3
+        src = O.at[(2 * t + u) * 8 + w]
+        dst = att.at[head, spot]
+        copy = pltpu.make_async_remote_copy(
+            src_ref=src,
+            dst_ref=dst,
+            send_sem=gs.at[(2 * t + u) * 8 + w],
+            recv_sem=gr,
+            device_id={"sp": to_sp, "tp": to_tp},
+            device_id_type=MESH,
+        )
+        return (to_sp == me) & (to_tp == tp), copy, src, dst
+
     for t in range(NT):
-        c = chunk_of(t, mm)
-        nb = lax.div(c * QW + QW - 1, BL) + 1
-        qk(0, t, S0, mx0)
-        mask(0, c, S0, mx0)
-
-        def body(i, _):
-            b = 2 * i
-            nxt = jnp.minimum(b + 1, nb - 1)
-            qk(nxt, t, S1, mx1)
-            pv(b, t, S0, mx0)
-            mask(nxt, c, S1, mx1)
-
-            @pl.when(b + 1 < nb)
-            def _():
-                after = jnp.minimum(b + 2, nb - 1)
-                qk(after, t, S0, mx0)
-                pv(b + 1, t, S1, mx1)
-                mask(after, c, S0, mx0)
-
-            return 0
-
-        lax.fori_loop(0, lax.div(nb + 1, 2), body, 0)
         a = A[t]
-        o_ref[t] = (a[16:80] / a[0:1]).T.astype(jnp.bfloat16)
-
-
-def attention(member, kvl, qt):
+        out = (a[16:80] / a[0:1]).T.astype(jnp.bfloat16)
+        for n in range(16):
+            O[16 * t + n] = jnp.concatenate(
+                [out[32 * n : 32 * n + 16], out[32 * n + 16 : 32 * n + 32]], axis=1
+            )
+    for t in range(NT):
+        for u in range(2):
+
+            def send(w, _):
+                mine, copy, src, dst = piece(t, u, w)
+
+                @pl.when(jnp.logical_not(mine))
+                def _():
+                    copy.start()
+
+                @pl.when(mine)
+                def _():
+                    pltpu.make_async_copy(src, dst, gr).start()
+
+                return 0
+
+            lax.fori_loop(0, 8, send, 0)
+    for t in range(NT):
+        for u in range(2):
+
+            def sent(w, _):
+                mine, copy, src, dst = piece(t, u, w)
+
+                @pl.when(jnp.logical_not(mine))
+                def _():
+                    copy.wait_send()
+
+                return 0
+
+            lax.fori_loop(0, 8, sent, 0)
+    gather.finish()
+    keep.wait()
+    for copy in sends:
+        copy.wait_send()
+    for to, copy in qsends:
+
+        @pl.when(to != me)
+        def _():
+            copy.wait_send()
+
+    pltpu.make_async_copy(att, att, gr).wait()
+
+
+def attend(q, k, v, gates, w):
     return pl.pallas_call(
-        attention_kernel,
-        name="attention",
-        out_shape=jax.ShapeDtypeStruct((NT, QW, HD), jnp.bfloat16),
-        in_specs=[pl.BlockSpec(memory_space=pltpu.SMEM), VMEM, VMEM],
-        out_specs=VMEM,
+        attend_kernel,
+        name="attend",
+        out_shape=(
+            jax.ShapeDtypeStruct((32, 3, 16, 128), jnp.bfloat16),
+            jax.ShapeDtypeStruct((8, 256, 2048), jnp.bfloat16),
+        ),
+        in_specs=[VMEM] * 4 + [ANY],
+        out_specs=(ANY, ANY),
         scratch_shapes=[
-            pltpu.VMEM((NB * BL, 128), jnp.bfloat16),
+            pltpu.VMEM((NB, KVR, BL), jnp.bfloat16),
+            pltpu.VMEM((2 * NT, HD, 256), jnp.bfloat16),
+            pltpu.VMEM((4, KVR, BL), jnp.bfloat16),
+            pltpu.VMEM((12, HD, 256), jnp.bfloat16),
+            pltpu.VMEM((256, 2048), jnp.bfloat16),
+            pltpu.VMEM((BL, 128), jnp.bfloat16),
             pltpu.VMEM((NT, 256, QW), jnp.bfloat16),
             pltpu.VMEM((BL, QW), jnp.float32),
             pltpu.VMEM((BL, QW), jnp.float32),
@@ -353,86 +420,100 @@
             pltpu.VMEM((8, QW), jnp.float32),
             pltpu.VMEM((NT, 8, QW), jnp.float32),
             pltpu.VMEM((NT, 80, QW), jnp.float32),
-            pltpu.VMEM((NB, 8, 128), jnp.float32),
+            pltpu.VMEM((96, 16, 128), jnp.bfloat16),
+            pltpu.SemaphoreType.DMA((16,)),
+            pltpu.SemaphoreType.DMA((16,)),
+            pltpu.SemaphoreType.DMA((12,)),
+            pltpu.SemaphoreType.DMA((12,)),
+            pltpu.SemaphoreType.DMA((9,)),
+            pltpu.SemaphoreType.DMA((8, 2)),
+            pltpu.SemaphoreType.DMA((2,)),
+            pltpu.SemaphoreType.DMA((96,)),
+            pltpu.SemaphoreType.DMA,
         ],
-        compiler_params=pltpu.CompilerParams(vmem_limit_bytes=48 * 2**20),
-        cost_estimate=pl.CostEstimate(flops=40 * 10**9, bytes_accessed=8 * 10**6, transcendentals=0),
-    )(member, kvl, qt)
-
-
-def give_back_kernel(o_ref, att, ss, rs):
+        compiler_params=pltpu.CompilerParams(
+            collective_id=0, has_side_effects=True, vmem_limit_bytes=48 * 2**20
+        ),
+        cost_estimate=pl.CostEstimate(flops=90 * 10**9, bytes_accessed=8 * 10**6, transcendentals=0),
+    )(q, k, v, gates, w)
+
+
+class GridGather:
+    def __init__(self, own, buf, send, recv):
+        self.own, self.buf, self.send, self.recv = own, buf, send, recv
+        self.half = buf.shape[0] // 2
+        self.width = buf.shape[1] // 16
+
+    def view(self, part, first, blocks=1):
+        lanes = pl.ds(pl.multiple_of(first * self.width, self.width), blocks * self.width)
+        return self.buf.at[pl.ds(part * self.half, self.half), lanes]
+
+    def copy(self, n, src, dst, to):
+        return pltpu.make_async_remote_copy(
+            src_ref=src,
+            dst_ref=dst,
+            send_sem=self.send.at[n],
+            recv_sem=self.recv.at[n],
+            device_id={"sp": to},
+            device_id_type=MESH,
+        )
+
+    def first(self):
+        me = lax.axis_index("sp")
+        z, y = me // 4, me % 4
+        out = []
+        for d in (1, 3, 2):
+            to = (z * 4 + (y + d) % 4, ((z + d) % 4) * 4 + y)
+            for part in range(2):
+                src = self.own.at[pl.ds(part * self.half, self.half)]
+                out.append(self.copy(2 * d + part, src, self.view(part, me), to[part]))
+        return out
+
+    def second(self):
+        me = lax.axis_index("sp")
+        z, y = me // 4, me % 4
+        out = []
+        for d in (1, 3, 2):
+            strip = self.view(0, 4 * z, 4)
+            out.append(self.copy(8 + d, strip, strip, ((z + d) % 4) * 4 + y))
+            for k in range(4):
+                one = self.view(1, 4 * k + y)
+                out.append(self.copy(12 + 4 * (d - 1) + k, one, one, z * 4 + (y + d) % 4))
+        return out
+
+
+def mix_kernel(
+    att, w_ref, stream, gain, bias, dw, out, wd, lhs, wbuf, res,
+    ws, rs, send, recv, ds, dr,
+):
+    tp = lax.axis_index("tp")
     me = lax.axis_index("sp")
-    tp = lax.axis_index("tp")
-    member = member_of(me)
-    head = tp * 4 + head_of(me)
-    for phase in range(2):
-        for t in range(NT):
-            c = chunk_of(t, member)
-            for u in range(2):
-                sub = 2 * c + u
-
-                def one(w, _):
-                    to_sp = sub // 3
-                    piece = 8 * (sub % 3) + w
-                    to_tp = piece // 3
-                    spot = 32 * (piece % 3)
-                    src = o_ref.at[t, pl.ds(pl.multiple_of(256 * u + 32 * w, 32), 32)]
-                    dst = att.at[head, pl.ds(pl.multiple_of(spot, 32), 32)]
-                    n = (2 * t + u) * 8 + w
-                    copy = pltpu.make_async_remote_copy(
-                        src_ref=src,
-                        dst_ref=dst,
-                        send_sem=ss.at[n],
-                        recv_sem=rs,
-                        device_id={"sp": to_sp, "tp": to_tp},
-                        device_id_type=MESH,
-                    )
-                    mine = (to_sp == me) & (to_tp == tp)
-
-                    @pl.when(jnp.logical_not(mine))
-                    def _():
-                        if phase == 0:
-                            copy.start()
-                        else:
-                            copy.wait_send()
-
-                    if phase == 0:
-
-                        @pl.when(mine)
-                        def _():
-                            pltpu.make_async_copy(src, dst, rs).start()
-
-                    return 0
-
-                lax.fori_loop(0, 8, one, 0)
-    pltpu.make_async_copy(att, att, rs).wait()
-
-
-def give_back(o):
-    return pl.pallas_call(
-        give_back_kernel,
-        name="give_back",
-        out_shape=jax.ShapeDtypeStruct((32, 96, HD), jnp.bfloat16),
-        in_specs=[VMEM],
-        out_specs=ANY,
-        scratch_shapes=[pltpu.SemaphoreType.DMA((96,)), pltpu.SemaphoreType.DMA],
-        compiler_params=pltpu.CompilerParams(has_side_effects=True),
-        cost_estimate=pl.CostEstimate(flops=10 * 10**9, bytes_accessed=10**6, transcendentals=0),
-    )(o)
-
-
-def mix_kernel(att, w_ref, stream, gain, bias, out, lhs, wbuf, res, ws, rs, send, recv):
-    tp = lax.axis_index("tp")
+    z, y = me // 4, me % 4
     greet_ring()
+    barrier = pltpu.get_barrier_semaphore()
+    for d in (1, 2, 3):
+        for to in (z * 4 + (y + d) % 4, ((z + d) % 4) * 4 + y):
+            pl.semaphore_signal(barrier, inc=1, device_id={"sp": to}, device_id_type=MESH)
     loads = [pltpu.make_async_copy(w_ref.at[j], wbuf.at[j], ws.at[j]) for j in range(8)]
     for load in loads:
         load.start()
     own = pltpu.make_async_copy(
-        stream.at[pl.ds(pl.multiple_of(tp * 96, 96), 96)], res, rs
+        stream.at[pl.ds(pl.multiple_of(tp * 96, 96), 96)], res, rs.at[0]
     )
     own.start()
+    keep = pltpu.make_async_copy(
+        dw, wd.at[:, pl.ds(pl.multiple_of(me * 128, 128), 128)], rs.at[1]
+    )
+    keep.start()
+    pl.semaphore_wait(barrier, 9)
+    down = GridGather(dw, wd, ds, dr)
+    one = down.first()
+    for copy in one:
+        copy.start()
     for h in range(32):
-        lhs[:, HD * h : HD * h + HD] = att[h]
+        for n in range(3):
+            lhs[32 * n : 32 * n + 16, HD * h : HD * h + HD] = att[h, n, :, 0:64]
+            lhs[32 * n + 16 : 32 * n + 32, HD * h : HD * h + HD] = att[h, n, :, 64:128]
     total = None
     for j in range(8):
         loads[j].wait()
@@ -444,32 +525,46 @@
     mixed = total.astype(jnp.bfloat16).astype(jnp.float32)
     p = ALPHA * res[...].astype(jnp.float32) + mixed
     out[tp] = layer_norm(p, gain[...], bias[...]).astype(jnp.bfloat16)
-    pl.semaphore_wait(pltpu.get_barrier_semaphore(), 3)
     gather = RingGather(out.at[tp], out, send, recv)
     gather.begin()
+    keep.wait()
+    for copy in one:
+        copy.wait_recv()
+    two = down.second()
+    for copy in two:
+        copy.start()
     gather.relay()
     gather.finish()
-
-
-def mix(att, w, stream, gain, bias):
+    for copy in two:
+        copy.wait_recv()
+    for copy in one + two:
+        copy.wait_send()
+
+
+def mix(att, w, stream, gain, bias, dw):
     return pl.pallas_call(
         mix_kernel,
         name="mix",
-        out_shape=jax.ShapeDtypeStruct((8, 96, 2048), jnp.bfloat16),
-        in_specs=[VMEM, ANY, ANY, VMEM, VMEM],
-        out_specs=VMEM,
+        out_shape=(
+            jax.ShapeDtypeStruct((8, 96, 2048), jnp.bfloat16),
+            jax.ShapeDtypeStruct((704, 2048), jnp.bfloat16),
+        ),
+        in_specs=[VMEM, ANY, ANY, VMEM, VMEM, VMEM],
+        out_specs=(VMEM, VMEM),
         scratch_shapes=[
             pltpu.VMEM((96, 2048), jnp.bfloat16),
             pltpu.VMEM((8, 256, 2048), jnp.bfloat16),
             pltpu.VMEM((96, 2048), jnp.bfloat16),
             pltpu.SemaphoreType.DMA((8,)),
-            pltpu.SemaphoreType.DMA,
+            pltpu.SemaphoreType.DMA((2,)),
             pltpu.SemaphoreType.DMA((9,)),
             pltpu.SemaphoreType.DMA((8, 2)),
+            pltpu.SemaphoreType.DMA((24,)),
+            pltpu.SemaphoreType.DMA((24,)),
         ],
         compiler_params=pltpu.CompilerParams(collective_id=1, has_side_effects=True),
         cost_estimate=pl.CostEstimate(flops=20 * 10**9, bytes_accessed=10**7, transcendentals=0),
-    )(att, w, stream, gain, bias)
+    )(att, w, stream, gain, bias, dw)
 
 
 def ffn_kernel(
@@ -608,14 +703,11 @@
     ffn_gain,
     ffn_bias,
 ):
-    member = member_of(lax.axis_index("sp")).astype(jnp.int32).reshape(1)
-    kvl, qt, wall = exchange(queries, key_rows, value_rows, log_forget.T, out_weight)
-    att = give_back(attention(member, kvl, qt))
-    normed = mix(att, wall, stream_in, mix_gain[None], mix_bias[None])
+    att, wall = attend(queries, key_rows, value_rows, log_forget.T, out_weight)
+    normed, down = mix(att, wall, stream_in, mix_gain[None], mix_bias[None], down_weight)
     both = lax.all_gather(
         jnp.concatenate([gate_weight, up_weight], axis=1), "sp", axis=0, tiled=True
     )
-    down = lax.all_gather(down_weight, "sp", axis=1, tiled=True)
     return ffn(normed.reshape(768, 2048), both, down, ffn_gain[None], ffn_bias[None])
 
 

time: 221 us -> 189 us (0.86)
  Pallas kernels: 187 us -> 164 us
  waiting for transfers between devices: 10.7 us -> 0.04 us
    pallas_call x4 -> x2, Pallas kernels: 156 us -> 133 us  [the longest x1 99 us: attend(): pl.pallas_call(attend_kernel, name='attend', out_shape=(jax.ShapeDtypeStr...]
    all_gather x1, waiting for transfers between devices: 9.96 us -> 0.02 us  [body(): lax.all_gather(jnp.concatenate([gate_weight, up_weight], axis=1), 'sp', a...]
    unnamed x9 -> x15, local copies, waits for them, and re-layouts: 7.74 us -> 9.53 us
  transfers between devices with their start and end apart: 2 -> 1, of which waited for: 1 -> 0; matrix products, arithmetic and copies ran while one was open for 1% -> 0% of each run, Pallas kernels for 71% -> 71%
where the time goes in v3:
time: 189 us; the launch traced here: 188 us
  Pallas kernels  164 us (87%)
  between operations  13.5 us (7%)
  local copies, waits for them, and re-layouts  9.53 us (5%)
    pallas_call x1, Pallas kernels, attend(): pl.pallas_call(attend_kernel, name='attend', out_shape=(jax.ShapeDtypeStr...  99 us
    pallas_call x1, Pallas kernels, mix(): pl.pallas_call(mix_kernel, name='mix', out_shape=(jax.ShapeDtypeStruct((8...  34.3 us
    pallas_call x1, Pallas kernels, ffn(): pl.pallas_call(ffn_kernel, name='ffn', out_shape=jax.ShapeDtypeStruct((96...  31.1 us
    unnamed x15, local copies, waits for them, and re-layouts  9.53 us
  transfers between devices with their start and end apart: 1, of which 0 were waited for; matrix products, arithmetic and copies ran while one was open for 0% of the time, Pallas kernels for 71%

profile of v3, /device:TPU:0, one launch (start us, length us, event | category | flops | bytes accessed | tf_op | source)
XLA Modules:
  0.0 188.2 jit_solution(13942342816725636780)
XLA Ops:
  6.5 0.0 all-gather.2.cloned.1.call-start
  6.5 1.1 copy.14
  7.6 1.1 copy.15
  8.7 0.9 pad_maximum_fusion
  9.5 0.0 all-gather.2.cloned.1.call-update
  9.5 0.0 copy-start
  9.5 1.2 copy-done
  10.8 0.0 copy-start.1
  10.8 1.0 copy-done.1
  11.8 0.0 copy-start.2
  11.8 1.0 copy-done.2
  12.8 0.0 copy-start.3
  12.8 1.0 copy-done.3
  13.8 0.0 copy-start.4
  13.8 0.7 copy-done.4
  14.5 99.0 %attend.1 = (bf16[32,3,16,128]{3,2,1,0:T(8,128)(2,1)S(1)}, bf16[8,256,2048]{2,1,0:T(8,128)(2,1)}) custom-call(bf16[768,256]{1,0:T(8,128)(2,1)S(1)} %copy-done.1, bf16[768,256]{1,0:T(8,128)(2,1)S(1)} %copy-done.2, bf16[768,256]{1,0:T(8,128)(2,1)S(1)} %copy-done.3, f32[4,768]{1,0:T(4,128)S(1)} %bitcast.6, bf16[256,2048]{1,0:T(8,128)(2,1)S(1)} %copy-done), custom_call_target="tpu_custom_call" | custom-call | flops 89999998976 | bytes 8000000 | tf_op jit(solution)/shard_map/attend/pallas_call | solution.py:400
  113.4 0.0 copy-start.5
  113.4 0.7 copy-done.5
  114.2 34.3 %mix.1 = (bf16[8,96,2048]{2,1,0:T(8,128)(2,1)}, bf16[704,2048]{1,0:T(8,128)(2,1)}) custom-call(bf16[32,3,16,128]{3,2,1,0:T(8,128)(2,1)} %copy-done.5, bf16[8,256,2048]{2,1,0:T(8,128)(2,1)} %get-tuple-element.10.w_ref, bf16[768,2048]{1,0:T(8,128)(2,1)} %stream.1, f32[1,2048]{1,0:T(1,128)} %bitcast.7, f32[1,2048]{1,0:T(1,128)} %bitcast.8, bf16[704,128]{1,0:T(8,128)(2,1)} %dw.1), custom_call_target="tpu_custom_call" | custom-call | flops 20000000000 | bytes 10000000 | tf_op jit(solution)/shard_map/mix/pallas_call | solution.py:545
  148.5 0.0 all-gather.2.cloned.1.call-done.both
  148.5 31.1 %ffn.1 = bf16[96,2048]{1,0:T(8,128)(2,1)} custom-call(bf16[768,2048]{1,0:T(8,128)(2,1)} %bitcast.11, bf16[2048,1408]{1,0:T(8,128)(2,1)} %all-gather.2.cloned.1.call-done.both, bf16[704,2048]{1,0:T(8,128)(2,1)} %get-tuple-element.12.down, f32[1,2048]{1,0:T(1,128)} %bitcast.9, f32[1,2048]{1,0:T(1,128)} %bitcast.10), custom_call_target="tpu_custom_call" | custom-call | flops 20000000000 | bytes 10000000 | tf_op jit(solution)/shard_map/ffn/pallas_call | solution.py:665
  179.6 1.8 copy.17
Async XLA Ops:
  6.5 142.0 %all-gather.2.cloned.1.call-start = ((), (), s32[]{:S(2)}) async-start(), calls=%async_computation | async-start | bytes 6127616 | tf_op jit(solution)/shard_map/all_gather | solution.py:708
  9.5 1.2 copy-start
  10.8 1.0 copy-start.1
  11.8 1.0 copy-start.2
  12.8 1.0 copy-start.3
  13.8 0.7 copy-start.4
  113.4 0.7 copy-start.5
Sparse Core Ops, SparseCore 0:
  9.7 109.2 all-gather.1

commit v4 on v3

v4 whole, which is shorter than its diff:
```python
import functools

import jax
import jax.numpy as jnp
from jax import lax
from jax.experimental import pallas as pl
from jax.experimental.pallas import tpu as pltpu
from jax.sharding import PartitionSpec as P

ALPHA = 8.0**0.25
EPSILON = 1e-05
MESH = pl.DeviceIdType.MESH
LOG2E = 1.4426950408889634
NEG = -1e30
BL = 768
ORDER = tuple(range(1, 16))
RELAY = (8, 9, 14)
QW = 512
NT = 6
NB = 16
HD = 64
KVR = 144
VMEM = pl.BlockSpec(memory_space=pltpu.VMEM)
ANY = pl.BlockSpec(memory_space=pl.ANY)


def layer_norm(matrix, norm_gain, norm_shift):
    centred = matrix - jnp.mean(matrix, axis=-1, keepdims=True)
    spread = jnp.mean(centred * centred, axis=-1, keepdims=True)
    return centred * lax.rsqrt(spread + EPSILON) * norm_gain + norm_shift


def parts(x):
    hi = x.astype(jnp.bfloat16).astype(jnp.float32)
    rest = x - hi
    mid = rest.astype(jnp.bfloat16).astype(jnp.float32)
    return hi, mid, rest - mid


def head_of(sp):
    z, y = sp // 4, sp % 4
    return (z // 2) * 2 + y // 2


def member_of(sp):
    z, y = sp // 4, sp % 4
    return (z % 2) * 2 + y % 2


def place_of(head, member):
    z = (head // 2) * 2 + member // 2
    y = (head % 2) * 2 + member % 2
    return z * 4 + y


def chunk_of(t, member):
    return (t // 2) * 8 + (member if t % 2 == 0 else 7 - member)


def ring():
    tp = lax.axis_index("tp")
    x, core = tp // 2, tp % 2
    right = ((x + 1) % 4) * 2 + core
    left = ((x + 3) % 4) * 2 + core
    far = ((x + 2) % 4) * 2 + core
    return tp, x * 2 + 1 - core, right, left, far


def greet_ring():
    tp, sibling, right, left, far = ring()
    barrier = pltpu.get_barrier_semaphore()
    for peer in (sibling, right, left):
        pl.semaphore_signal(barrier, inc=1, device_id={"tp": peer}, device_id_type=MESH)


class RingGather:
    def __init__(self, own, buf, send, recv):
        self.own, self.buf, self.send, self.recv = own, buf, send, recv
        self.rows = buf.shape[1]
        self.half = self.rows // 2
        self.count = 0

    def push(self, src, slot, peer, half=None):
        if half is None:
            dst, sem = self.buf.at[slot], self.recv.at[slot, 0]
        else:
            cut = pl.ds(half * self.half, self.half)
            dst, sem = self.buf.at[slot, cut], self.recv.at[slot, half]
        copy = pltpu.make_async_remote_copy(
            src_ref=src,
            dst_ref=dst,
            send_sem=self.send.at[self.count],
            recv_sem=sem,
            device_id={"tp": peer},
            device_id_type=MESH,
        )
        copy.start()
        self.count += 1

    def part(self, slot, half):
        return self.buf.at[slot, pl.ds(half * self.half, self.half)]

    def arrive(self, slot, half=None):
        if half is None:
            ref, sem = self.buf.at[slot], self.recv.at[slot, 0]
        else:
            ref, sem = self.part(slot, half), self.recv.at[slot, half]
        pltpu.make_async_copy(ref, ref, sem).wait()

    def begin(self):
        tp, sibling, right, left, far = ring()
        self.count = 0
        self.push(self.own, tp, right)
        self.push(self.own, tp, left)
        self.push(self.own, tp, sibling)

    def stage(self, n):
        tp, sibling, right, left, far = ring()
        self.count = 3 + 2 * n
        if n == 0:
            self.arrive(left)
            self.push(self.part(left, 0), left, right, 0)
            self.push(self.buf.at[left], left, sibling)
        elif n == 1:
            self.arrive(right)
            self.push(self.part(right, 1), right, left, 1)
            self.push(self.buf.at[right], right, sibling)
        else:
            for half in range(2):
                self.arrive(far, half)
                self.push(self.part(far, half), far, sibling, half)

    def relay(self):
        for n in range(3):
            self.stage(n)

    def finish(self):
        tp, sibling, right, left, far = ring()
        x = tp // 2
        other = 1 - tp % 2
        self.arrive(sibling)
        self.arrive(((x + 3) % 4) * 2 + other)
        self.arrive(((x + 1) % 4) * 2 + other)
        for half in range(2):
            self.arrive(((x + 2) % 4) * 2 + other, half)

    def sent(self):
        for n in range(9):
            ref = self.own if n not in (3, 5, 7, 8) else self.part(0, 0)
            pltpu.make_async_copy(ref, ref, self.send.at[n]).wait()


def greet_all():
    me = lax.axis_index("sp")
    tp = lax.axis_index("tp")
    barrier = pltpu.get_barrier_semaphore()

    def one(i, _):
        sp = (me + i // 8) % 16
        to = (tp + i % 8) % 8
        pl.semaphore_signal(
            barrier, inc=1, device_id={"sp": sp, "tp": to}, device_id_type=MESH
        )
        return 0

    lax.fori_loop(1, 128, one, 0)


class GridGather:
    def __init__(self, buf, send, recv):
        self.buf, self.send, self.recv = buf, send, recv

    def view(self, phase, part, k, half=None):
        me = lax.axis_index("sp")
        z, y = me // 4, me % 4
        tail = (part,) if half is None else (part, half)
        if phase == 0:
            return self.buf.at[(z, k) + tail] if part == 0 else self.buf.at[(k, y) + tail]
        every = pl.ds(0, 4)
        return self.buf.at[(k, every) + tail] if part == 0 else self.buf.at[(every, k) + tail]

    def ring(self, phase, part):
        me = lax.axis_index("sp")
        z, y = me // 4, me % 4
        along_y = phase == part
        at = y if along_y else z
        right, left = (at + 1) % 4, (at + 3) % 4
        if along_y:
            return at, right, left, z * 4 + right, z * 4 + left
        return at, right, left, right * 4 + y, left * 4 + y

    def copies(self, phase, part):
        at, right, left, to_right, to_left = self.ring(phase, part)

        def one(n, view, to):
            return pltpu.make_async_remote_copy(
                src_ref=view,
                dst_ref=view,
                send_sem=self.send.at[phase, part, n],
                recv_sem=self.recv.at[phase, part, n],
                device_id={"sp": to},
                device_id_type=MESH,
            )

        return (
            one(0, self.view(phase, part, at), to_right),
            one(1, self.view(phase, part, at), to_left),
            one(2, self.view(phase, part, left, 0), to_right),
            one(3, self.view(phase, part, right, 1), to_left),
        )

    def begin(self, phase):
        for part in range(2):
            copies = self.copies(phase, part)
            copies[0].start()
            copies[1].start()

    def relay(self, phase):
        for part in range(2):
            copies = self.copies(phase, part)
            copies[0].wait_recv()
            copies[2].start()
            copies[1].wait_recv()
            copies[3].start()

    def finish(self, phase):
        for part in range(2):
            copies = self.copies(phase, part)
            copies[2].wait_recv()
            copies[3].wait_recv()

    def sent(self):
        for phase in range(2):
            for part in range(2):
                for copy in self.copies(phase, part):
                    copy.wait_send()


def layer_kernel(
    q_hbm, k_hbm, v_hbm, g_ref, w_ref, stream, gate_w, up_w, down_w, gain1, bias1, gain2, bias2,
    out,
    q_ref, k_ref, v_ref, att, wall, kvl, qt, ksrc, qsrc, X, R, S0, S1, mx0, mx1, M, A, O,
    G, D, rows, lhs, res, hid, pb, sib, zz, rel, inn,
    ks, kr, qs, qr, ws, wr, ld, gs, gr, Gs, Gr, Ds, Dr, ns, nr, ss, sr, hs, hr,
):
    me = lax.axis_index("sp")
    tp = lax.axis_index("tp")
    z, y = me // 4, me % 4
    greet_all()
    loads = [
        pltpu.make_async_copy(src, dst, ld.at[n])
        for n, (src, dst) in enumerate(
            (
                (k_hbm, k_ref),
                (v_hbm, v_ref),
                (q_hbm, q_ref),
                (w_ref, wall.at[tp]),
                (gate_w, G.at[z, y, :, 0]),
                (up_w, G.at[z, y, :, 1]),
                (down_w, D.at[z, y]),
                (stream.at[pl.ds(pl.multiple_of(tp * 96, 96), 96)], res),
            )
        )
    ]
    for load in loads:
        load.start()
    for load in loads[:3]:
        load.wait()
    kt = k_ref[...].T
    vt = v_ref[...].T
    qtt = q_ref[...].T
    gates = g_ref[...]
    row = lax.broadcasted_iota(jnp.int32, (16, BL), 0)
    for h in range(4):
        g = gates[h : h + 1]
        first = jnp.broadcast_to(g[:, 0:1], (1, BL))
        lines = [jnp.ones((1, BL), jnp.float32)]
        lines += parts((first - g) * LOG2E) + parts(first * (-LOG2E))
        extra = jnp.zeros((16, BL), jnp.float32)
        for n, r in enumerate(lines):
            extra = jnp.where(row == n, r, extra)
        ksrc[h, 0:64] = kt[64 * h : 64 * h + 64]
        ksrc[h, 64:80] = extra.astype(jnp.bfloat16)
        ksrc[h, 80:144] = vt[64 * h : 64 * h + 64]
        for i in range(3):
            qsrc[3 * h + i] = qtt[64 * h : 64 * h + 64, 256 * i : 256 * i + 256]
    pl.semaphore_wait(pltpu.get_barrier_semaphore(), 127)
    qsends = []
    for h in range(4):
        for i in range(3):
            n = 3 * h + i
            sub = 3 * me + i
            c, u = sub // 2, sub % 2
            r = c % 8
            high = r // 4
            member = r + high * (7 - 2 * r)
            slot = 2 * ((c // 8) * 2 + high) + u
            to = place_of(h, member)
            copy = pltpu.make_async_remote_copy(
                src_ref=qsrc.at[n],
                dst_ref=qt.at[slot],
                send_sem=qs.at[n],
                recv_sem=qr.at[slot],
                device_id={"sp": to},
                device_id_type=MESH,
            )
            local = pltpu.make_async_copy(qsrc.at[n], qt.at[slot], qr.at[slot])

            @pl.when(to != me)
            def _():
                copy.start()

            @pl.when(to == me)
            def _():
                local.start()

            qsends.append((to, copy))
    sends = []
    for o in ORDER:
        to = ((z + o // 4) % 4) * 4 + (y + o % 4) % 4
        copy = pltpu.make_async_remote_copy(
            src_ref=ksrc.at[head_of(to)],
            dst_ref=kvl.at[me],
            send_sem=ks.at[o],
            recv_sem=kr.at[me],
            device_id={"sp": to},
            device_id_type=MESH,
        )
        copy.start()
        sends.append(copy)
    own = pltpu.make_async_copy(ksrc.at[head_of(me)], kvl.at[me], kr.at[me])
    own.start()
    for load in loads[3:]:
        load.wait()
    gather = RingGather(wall.at[tp], wall, ws, wr)
    gather.begin()
    upper = GridGather(G, Gs, Gr)
    lower = GridGather(D, Ds, Dr)
    upper.begin(0)
    lower.begin(0)

    row = lax.broadcasted_iota(jnp.int32, (64, QW), 0)
    ones = jnp.where((row >= 1) & (row < 4), 1.0, 0.0).astype(jnp.bfloat16)
    for t in range(NT):
        for u in range(2):
            pltpu.make_async_copy(qsrc.at[0], qt.at[2 * t + u], qr.at[2 * t + u]).wait()
        q = jnp.concatenate([qt[2 * t], qt[2 * t + 1]], axis=1).astype(jnp.float32)
        q = q * (LOG2E / 8)
        hi = q.astype(jnp.bfloat16)
        R[t, 0:64] = hi
        R[t, 64:128] = ones
        R[t, 128:192] = (q - hi.astype(jnp.float32)).astype(jnp.bfloat16)
        R[t, 192:256] = jnp.zeros((64, QW), jnp.bfloat16)
        M[t] = jnp.full((8, QW), NEG, jnp.float32)
        A[t] = jnp.zeros((80, QW), jnp.float32)

    mm = member_of(me)
    S = (S0, S1)
    mx = (mx0, mx1)

    def qk(t, n):
        x = X[...]
        s = jnp.dot(
            jnp.concatenate([x, x], axis=1), R[t], preferred_element_type=jnp.float32
        )
        S[n][...] = s
        mx[n][...] = jnp.max(s.reshape(BL // 8, 8, QW), axis=0)

    def mask(b, t, n):
        c = chunk_of(t, mm)

        @pl.when(b * BL + BL > c * QW)
        def _():
            kp = b * BL + lax.broadcasted_iota(jnp.int32, (BL, QW), 0)
            qp = c * QW + lax.broadcasted_iota(jnp.int32, (BL, QW), 1)
            s = jnp.where(kp <= qp, S[n][...], NEG)
            S[n][...] = s
            mx[n][...] = jnp.max(s.reshape(BL // 8, 8, QW), axis=0)

    def pv(b, t, n, bs):
        m_old = M[t][0:1]
        m_new = jnp.maximum(m_old, jnp.max(mx[n][...], axis=0, keepdims=True) + bs)
        p = jnp.exp2(S[n][...] - (m_new - bs)).astype(jnp.bfloat16)
        o = jnp.dot(kvl[b, 64:144], p, preferred_element_type=jnp.float32)
        A[t] = A[t] * jnp.exp2(m_old - m_new) + o
        M[t] = jnp.broadcast_to(m_new, (8, QW))

    def block(i, _):
        o = i
        b = ((z + 4 - o // 4) % 4) * 4 + (y + 4 - o % 4) % 4
        pltpu.make_async_copy(ksrc.at[0], kvl.at[b], kr.at[b]).wait()
        X[...] = kvl[b, 0:128, :].T
        g = kvl[b, 64:80, 0:128].astype(jnp.float32)
        bs = jnp.tile(g[4:5] + g[5:6] + g[6:7], (1, QW // 128))

        def live(t):
            return chunk_of(t, mm) * QW + QW > b * BL

        for t in range(NT):
            first = live(t) if t == 0 else live(t) & jnp.logical_not(live(t - 1))

            @pl.when(first)
            def _():
                qk(t, t % 2)
                mask(b, t, t % 2)

            @pl.when(live(t))
            def _():
                if t + 1 < NT:
                    qk(t + 1, (t + 1) % 2)
                pv(b, t, t % 2, bs)
                if t + 1 < NT:
                    mask(b, t + 1, (t + 1) % 2)

        for stage in range(3):

            @pl.when(i == RELAY[stage])
            def _():
                gather.stage(stage)

        return 0

    lax.fori_loop(0, 16, block, 0)

    head = tp * 4 + head_of(me)

    def piece(t, u, w):
        sub = 2 * chunk_of(t, mm) + u
        n = 8 * (sub % 3) + w
        to_sp, to_tp, spot = sub // 3, n // 3, n % 3
        src = O.at[(2 * t + u) * 8 + w]
        dst = att.at[head, spot]
        copy = pltpu.make_async_remote_copy(
            src_ref=src,
            dst_ref=dst,
            send_sem=gs.at[(2 * t + u) * 8 + w],
            recv_sem=gr,
            device_id={"sp": to_sp, "tp": to_tp},
            device_id_type=MESH,
        )
        return (to_sp == me) & (to_tp == tp), copy, src, dst

    for t in range(NT):
        a = A[t]
        heads = (a[16:80] / a[0:1]).T.astype(jnp.bfloat16)
        for n in range(16):
            O[16 * t + n] = jnp.concatenate(
                [heads[32 * n : 32 * n + 16], heads[32 * n + 16 : 32 * n + 32]], axis=1
            )
    for t in range(NT):
        for u in range(2):

            def send(w, _):
                mine, copy, src, dst = piece(t, u, w)

                @pl.when(jnp.logical_not(mine))
                def _():
                    copy.start()

                @pl.when(mine)
                def _():
                    pltpu.make_async_copy(src, dst, gr).start()

                return 0

            lax.fori_loop(0, 8, send, 0)
    upper.relay(0)
    lower.relay(0)
    upper.finish(0)
    upper.begin(1)
    lower.finish(0)
    lower.begin(1)
    gather.finish()
    pltpu.make_async_copy(att, att, gr).wait()
    for h in range(32):
        for n in range(3):
            lhs[32 * n : 32 * n + 16, HD * h : HD * h + HD] = att[h, n, :, 0:64]
            lhs[32 * n + 16 : 32 * n + 32, HD * h : HD * h + HD] = att[h, n, :, 64:128]
    mixed = jnp.dot(
        lhs[...], wall[...].reshape(2048, 2048), preferred_element_type=jnp.float32
    )
    mixed = mixed.astype(jnp.bfloat16).astype(jnp.float32)
    p = ALPHA * res[...].astype(jnp.float32) + mixed
    rows[tp] = layer_norm(p, gain1[...], bias1[...]).astype(jnp.bfloat16)
    spread = RingGather(rows.at[tp], rows, ns, nr)
    spread.begin()
    upper.relay(1)

    x, core = tp // 2, tp % 2
    _, sibling, right, left, far = ring()

    def project(chip):
        r = rows[pl.ds(2 * chip, 2)].reshape(192, 2048)
        gate = jnp.dot(
            r, G[:, :, :, 0].reshape(2048, 704), preferred_element_type=jnp.float32
        )
        up = jnp.dot(
            r, G[:, :, :, 1].reshape(2048, 704), preferred_element_type=jnp.float32
        )
        hid[chip] = (gate / (1.0 + jnp.exp(-gate)) * up).astype(jnp.bfloat16)

    other = 1 - core
    spread.stage(0)
    spread.stage(1)
    upper.finish(1)
    lower.relay(1)
    spread.arrive(sibling)
    chips = ((x + 2) % 4, (x + 1) % 4, (x + 3) % 4, x)

    def early(n, _):
        chip = (x + n - n // 2 + n % 2 * (1 - n // 2) * 2) % 4
        project(chip)

        @pl.when(n == 0)
        def _():
            spread.stage(2)
            spread.arrive(chips[2] * 2 + other)
            spread.arrive(chips[1] * 2 + other)

        @pl.when(n == 2)
        def _():
            for half in range(2):
                spread.arrive(chips[0] * 2 + other, half)

        return 0

    lax.fori_loop(0, 4, early, 0)
    lower.finish(1)

    def to_sibling(n):
        return pltpu.make_async_remote_copy(
            src_ref=pb.at[n, other],
            dst_ref=sib.at[n],
            send_sem=ss.at[n],
            recv_sem=sr.at[n],
            device_id={"tp": sibling},
            device_id_type=MESH,
        )

    def hop(n, src, dst, peer):
        return pltpu.make_async_remote_copy(
            src_ref=src,
            dst_ref=dst,
            send_sem=hs.at[n],
            recv_sem=hr.at[n],
            device_id={"tp": peer},
            device_id_type=MESH,
        )

    hops = [
        hop(0, zz.at[0, pl.ds(0, 48)], rel.at[0], right),
        hop(1, zz.at[0, pl.ds(48, 48)], rel.at[1], left),
        hop(2, zz.at[1], inn.at[0], right),
        hop(3, zz.at[2], inn.at[1], left),
    ]

    def product(n):
        wd = jnp.concatenate(
            [D[k // 4, k % 4].reshape(704, 128) for k in range(16)], axis=1
        )
        s = jnp.dot(hid[chips[n]], wd, preferred_element_type=jnp.float32)
        s = s.astype(jnp.bfloat16)
        pb[n, 0] = s[:96]
        pb[n, 1] = s[96:]
        to_sibling(n).start()

    def pair(n):
        to_sibling(n).wait_recv()
        return pb[n, core].astype(jnp.float32) + sib[n].astype(jnp.float32)

    product(0)
    product(1)
    zz[0] = pair(0).astype(jnp.bfloat16)
    hops[0].start()
    hops[1].start()
    product(2)
    s = pair(1)
    hops[0].wait_recv()
    zz[1, 0:48] = (s[:48] + rel[0].astype(jnp.float32)).astype(jnp.bfloat16)
    zz[1, 48:96] = s[48:].astype(jnp.bfloat16)
    hops[2].start()
    product(3)
    s = pair(2)
    hops[1].wait_recv()
    zz[2, 0:48] = s[:48].astype(jnp.bfloat16)
    zz[2, 48:96] = (s[48:] + rel[1].astype(jnp.float32)).astype(jnp.bfloat16)
    hops[3].start()
    s = pair(3)
    hops[2].wait_recv()
    hops[3].wait_recv()
    s = s + inn[0].astype(jnp.float32) + inn[1].astype(jnp.float32)
    lowered = s.astype(jnp.bfloat16).astype(jnp.float32)
    normed = rows[tp].astype(jnp.float32)
    out[...] = layer_norm(ALPHA * normed + lowered, gain2[...], bias2[...]).astype(jnp.bfloat16)
    for n in range(4):
        to_sibling(n).wait_send()
        hops[n].wait_send()
    spread.sent()
    upper.sent()
    lower.sent()
    for t in range(NT):
        for u in range(2):

            def sent(w, _):
                mine, copy, src, dst = piece(t, u, w)

                @pl.when(jnp.logical_not(mine))
                def _():
                    copy.wait_send()

                return 0

            lax.fori_loop(0, 8, sent, 0)
    gather.sent()
    for copy in sends:
        copy.wait_send()
    for to, copy in qsends:

        @pl.when(to != me)
        def _():
            copy.wait_send()


def layer(*args):
    bf = jnp.bfloat16
    dma = pltpu.SemaphoreType.DMA
    scratch = [
        pltpu.VMEM((BL, 256), bf),
        pltpu.VMEM((BL, 256), bf),
        pltpu.VMEM((BL, 256), bf),
        pltpu.VMEM((32, 3, 16, 128), bf),
        pltpu.VMEM((8, 256, 2048), bf),
        pltpu.VMEM((NB, KVR, BL), bf),
        pltpu.VMEM((2 * NT, HD, 256), bf),
        pltpu.VMEM((4, KVR, BL), bf),
        pltpu.VMEM((12, HD, 256), bf),
        pltpu.VMEM((BL, 128), bf),
        pltpu.VMEM((NT, 256, QW), bf),
        pltpu.VMEM((BL, QW), jnp.float32),
        pltpu.VMEM((BL, QW), jnp.float32),
        pltpu.VMEM((8, QW), jnp.float32),
        pltpu.VMEM((8, QW), jnp.float32),
        pltpu.VMEM((NT, 8, QW), jnp.float32),
        pltpu.VMEM((NT, 80, QW), jnp.float32),
        pltpu.VMEM((96, 16, 128), bf),
        pltpu.VMEM((4, 4, 2, 2, 64, 704), bf),
        pltpu.VMEM((4, 4, 2, 2, 176, 128), bf),
        pltpu.VMEM((8, 96, 2048), bf),
        pltpu.VMEM((96, 2048), bf),
        pltpu.VMEM((96, 2048), bf),
        pltpu.VMEM((4, 192, 704), bf),
        pltpu.VMEM((4, 2, 96, 2048), bf),
        pltpu.VMEM((4, 96, 2048), bf),
        pltpu.VMEM((3, 96, 2048), bf),
        pltpu.VMEM((2, 48, 2048), bf),
        pltpu.VMEM((2, 96, 2048), bf),
        dma((16,)), dma((16,)), dma((12,)), dma((12,)), dma((9,)), dma((8, 2)), dma((8,)),
        dma((96,)), dma, dma((2, 2, 4)), dma((2, 2, 4)), dma((2, 2, 4)), dma((2, 2, 4)),
        dma((9,)), dma((8, 2)), dma((4,)), dma((4,)), dma((4,)), dma((4,)),
    ]
    return pl.pallas_call(
        layer_kernel,
        name="layer",
        out_shape=jax.ShapeDtypeStruct((96, 2048), bf),
        in_specs=[ANY] * 3 + [VMEM] + [ANY] * 5 + [VMEM] * 4,
        out_specs=VMEM,
        scratch_shapes=scratch,
        compiler_params=pltpu.CompilerParams(
            collective_id=0, has_side_effects=True, vmem_limit_bytes=62 * 2**20
        ),
    )(*args)


def body(
    queries,
    key_rows,
    value_rows,
    log_forget,
    stream_in,
    out_weight,
    mix_gain,
    mix_bias,
    gate_weight,
    up_weight,
    down_weight,
    ffn_gain,
    ffn_bias,
):
    return layer(
        queries,
        key_rows,
        value_rows,
        log_forget.T,
        out_weight,
        stream_in,
        gate_weight.reshape(2, 64, 704),
        up_weight.reshape(2, 64, 704),
        down_weight.reshape(2, 2, 176, 128),
        mix_gain[None],
        mix_bias[None],
        ffn_gain[None],
        ffn_bias[None],
    )


def solution(mesh):
    placed = (
        P("sp", "tp"),
        P("sp", "tp"),
        P("sp", "tp"),
        P("sp", "tp"),
        P("sp", None),
        P("tp", None),
        P(),
        P(),
        P("sp", "tp"),
        P("sp", "tp"),
        P("tp", "sp"),
        P(),
        P(),
    )
    return jax.shard_map(
        body, mesh=mesh, in_specs=placed, out_specs=P(("sp", "tp"), None), check_vma=False
    )
```

time: 189 us -> 164 us (0.87)
  between operations: 13.5 us -> 0.01 us
  Pallas kernels: 164 us -> 159 us
  local copies, waits for them, and re-layouts: 9.53 us -> 5.23 us
    pallas_call x3 -> x1, Pallas kernels: 164 us -> 159 us  [layer(): pl.pallas_call(layer_kernel, name='layer', out_shape=jax.ShapeDtypeStruct...]
    unnamed x15 -> x3, local copies, waits for them, and re-layouts: 9.53 us -> 5.23 us
  transfers between devices with their start and end apart: 1 -> 0, of which waited for: 0 -> 0; matrix products, arithmetic and copies ran while one was open for 0% -> 0% of each run, Pallas kernels for 71% -> 0%
where the time goes in v4:
time: 164 us
  Pallas kernels  159 us (97%)
  local copies, waits for them, and re-layouts  5.23 us (3%)
    pallas_call x1, Pallas kernels, layer(): pl.pallas_call(layer_kernel, name='layer', out_shape=jax.ShapeDtypeStruct...  159 us
    unnamed x3, local copies, waits for them, and re-layouts  5.23 us

profile of v4, /device:TPU:0, one launch (start us, length us, event | category | flops | bytes accessed | tf_op | source)
XLA Modules:
  0.0 163.8 jit_solution(11457277678731620024)
XLA Ops:
  0.0 1.7 %copy.14 = bf16[128,704]{1,0:T(8,128)(2,1)} copy(bf16[128,704]{0,1:T(8,128)(2,1)} %param.21) | data formatting | bytes 360448 | tf_op args[8]
  1.7 1.7 %copy.15 = bf16[128,704]{1,0:T(8,128)(2,1)} copy(bf16[128,704]{0,1:T(8,128)(2,1)} %param.22) | data formatting | bytes 360448 | tf_op args[9]
  3.5 158.6 %layer.1 = bf16[96,2048]{1,0:T(8,128)(2,1)} custom-call(bf16[768,256]{1,0:T(8,128)(2,1)} %q_hbm.1, bf16[768,256]{1,0:T(8,128)(2,1)} %k_hbm.1, bf16[768,256]{1,0:T(8,128)(2,1)} %v_hbm.1, f32[4,768]{1,0:T(4,128)} %bitcast.11, bf16[256,2048]{1,0:T(8,128)(2,1)} %w_ref.1, bf16[768,2048]{1,0:T(8,128)(2,1)} %stream.1, bf16[2,64,704]{2,1,0:T(8,128)(2,1)} %bitcast.8, ...), custom_call_target="tpu_custom_call" | custom-call | tf_op jit(solution)/shard_map/layer/pallas_call | solution.py:661
  162.1 1.8 %copy.17 = bf16[96,2048]{1,0:T(8,128)(2,1)} copy(bf16[96,2048]{1,0:T(8,128)(2,1)} %layer.1) | data formatting | bytes 786432

commit v5 on v4

--- a/solution.py
+++ b/solution.py
@@ -13,8 +13,7 @@
 LOG2E = 1.4426950408889634
 NEG = -1e30
 BL = 768
-ORDER = tuple(range(1, 16))
-RELAY = (8, 9, 14)
+RELAY = (9, 10, 13)
 QW = 512
 NT = 6
 NB = 16
@@ -150,20 +149,16 @@
             pltpu.make_async_copy(ref, ref, self.send.at[n]).wait()
 
 
-def greet_all():
+def greet_lines():
     me = lax.axis_index("sp")
     tp = lax.axis_index("tp")
     barrier = pltpu.get_barrier_semaphore()
-
-    def one(i, _):
-        sp = (me + i // 8) % 16
-        to = (tp + i % 8) % 8
-        pl.semaphore_signal(
-            barrier, inc=1, device_id={"sp": sp, "tp": to}, device_id_type=MESH
-        )
-        return 0
-
-    lax.fori_loop(1, 128, one, 0)
+    for n in range(1, 16):
+        to = (me + n) % 16
+        pl.semaphore_signal(barrier, inc=1, device_id={"sp": to}, device_id_type=MESH)
+    for n in range(1, 8):
+        to = (tp + n) % 8
+        pl.semaphore_signal(barrier, inc=1, device_id={"tp": to}, device_id_type=MESH)
 
 
 class GridGather:
@@ -240,13 +235,13 @@
     q_hbm, k_hbm, v_hbm, g_ref, w_ref, stream, gate_w, up_w, down_w, gain1, bias1, gain2, bias2,
     out,
     q_ref, k_ref, v_ref, att, wall, kvl, qt, ksrc, qsrc, X, R, S0, S1, mx0, mx1, M, A, O,
-    G, D, rows, lhs, res, hid, pb, sib, zz, rel, inn,
-    ks, kr, qs, qr, ws, wr, ld, gs, gr, Gs, Gr, Ds, Dr, ns, nr, ss, sr, hs, hr,
+    G, D, rows, lhs, res, hid, pb, sib, zz, rel, inn, E, gt,
+    ks, kr, qs, qr, ws, wr, ld, gs, gr, Gs, Gr, Ds, Dr, ns, nr, ss, sr, hs, hr, er, line,
 ):
     me = lax.axis_index("sp")
     tp = lax.axis_index("tp")
     z, y = me // 4, me % 4
-    greet_all()
+    greet_lines()
     loads = [
         pltpu.make_async_copy(src, dst, ld.at[n])
         for n, (src, dst) in enumerate(
@@ -255,9 +250,12 @@
                 (v_hbm, v_ref),
                 (q_hbm, q_ref),
                 (w_ref, wall.at[tp]),
-                (gate_w, G.at[z, y, :, 0]),
-                (up_w, G.at[z, y, :, 1]),
-                (down_w, D.at[z, y]),
+                (gate_w, gt.at[0]),
+                (up_w, gt.at[1]),
+                (down_w.at[pl.ds(0, 176)], D.at[z, y, 0, 0]),
+                (down_w.at[pl.ds(176, 176)], D.at[z, y, 0, 1]),
+                (down_w.at[pl.ds(352, 176)], D.at[z, y, 1, 0]),
+                (down_w.at[pl.ds(528, 176)], D.at[z, y, 1, 1]),
                 (stream.at[pl.ds(pl.multiple_of(tp * 96, 96), 96)], res),
             )
         )
@@ -284,7 +282,10 @@
         ksrc[h, 80:144] = vt[64 * h : 64 * h + 64]
         for i in range(3):
             qsrc[3 * h + i] = qtt[64 * h : 64 * h + 64, 256 * i : 256 * i + 256]
-    pl.semaphore_wait(pltpu.get_barrier_semaphore(), 127)
+    pl.semaphore_wait(pltpu.get_barrier_semaphore(), 22)
+    for n in range(1, 16):
+        to = (me + n) % 16
+        pl.semaphore_signal(line, inc=1, device_id={"sp": to}, device_id_type=MESH)
     qsends = []
     for h in range(4):
         for i in range(3):
@@ -315,25 +316,108 @@
                 local.start()
 
             qsends.append((to, copy))
-    sends = []
-    for o in ORDER:
-        to = ((z + o // 4) % 4) * 4 + (y + o % 4) % 4
-        copy = pltpu.make_async_remote_copy(
-            src_ref=ksrc.at[head_of(to)],
-            dst_ref=kvl.at[me],
-            send_sem=ks.at[o],
-            recv_sem=kr.at[me],
+    own = pltpu.make_async_copy(ksrc.at[head_of(me)], kvl.at[me], kr.at[me])
+    own.start()
+    par = (z + y) % 2
+
+    def axes(cls):
+        return y + cls * (z - y), z + cls * (y - z)
+
+    def dev(cls, a, c):
+        return a * (1 + 3 * cls) + c * (4 - 3 * cls)
+
+    def half_head(cls, a, c):
+        return a * (1 + cls) + c * (2 - cls)
+
+    def mate(k):
+        return k + 1 - 2 * (k % 2)
+
+    def pass_on(n, src, dst, sem, to):
+        return pltpu.make_async_remote_copy(
+            src_ref=src,
+            dst_ref=dst,
+            send_sem=ks.at[n],
+            recv_sem=sem,
             device_id={"sp": to},
             device_id_type=MESH,
         )
-        copy.start()
-        sends.append(copy)
-    own = pltpu.make_async_copy(ksrc.at[head_of(me)], kvl.at[me], kr.at[me])
-    own.start()
+
+    a, c = axes(par)
+    ap, cp = a // 2, c // 2
+    mine = (kvl.at[me], kr.at[me])
+    side = (E.at[par, a], er.at[par, a])
+    for n, (head, (dst, sem), to) in enumerate(
+        (
+            (half_head(par, 1 - ap, 1 - cp), side, dev(par, 3 - a, c)),
+            (half_head(par, ap, 1 - cp), side, dev(par, mate(a), c)),
+            (half_head(par, 1 - ap, cp), mine, dev(par, 3 - a, c)),
+            (half_head(par, ap, cp), mine, dev(par, mate(a), c)),
+            (half_head(par, ap, 1 - cp), mine, dev(par, a, 3 - c)),
+            (half_head(par, ap, cp), mine, dev(par, a, mate(c))),
+        )
+    ):
+        pass_on(n, ksrc.at[head], dst, sem, to).start()
+
+    def fan(n, cls, b, slot):
+        a, c = axes(cls)
+        pltpu.make_async_copy(E.at[cls, slot], E.at[cls, slot], er.at[cls, slot]).wait()
+        pass_on(n, E.at[cls, slot], kvl.at[b], kr.at[b], dev(cls, a, 3 - c)).start()
+        pass_on(n + 1, kvl.at[b], kvl.at[b], kr.at[b], dev(cls, a, mate(c))).start()
+
+    def order(i):
+        j = jnp.maximum(i - 4, 0)
+        g, cls, f = j // 4, j % 4 // 2, j % 2
+        a, c = axes(cls)
+        far_c = jnp.where(g == 0, 3 - c, jnp.where(g == 1, mate(c), (c + 2) % 4))
+        late = dev(cls, (cls + far_c) % 2 + 2 * f, far_c)
+        ya, yc = axes(1 - par)
+        xa, xc = axes(par)
+        early = jnp.where(
+            i < 2,
+            jnp.where(i == 0, me, dev(1 - par, mate(ya), yc)),
+            jnp.where(i == 2, dev(1 - par, 3 - ya, yc), dev(par, (xa + 2) % 4, xc)),
+        )
+        return jnp.where(i < 4, early, late)
+
+    def arrive(i):
+        b = order(i)
+        pltpu.make_async_copy(ksrc.at[0], kvl.at[b], kr.at[b]).wait()
+
+        @pl.when(i == 1)
+        def _():
+            a, c = axes(1 - par)
+            fan(6, 1 - par, b, mate(a))
+
+        @pl.when(i == 2)
+        def _():
+            cls = 1 - par
+            a, c = axes(cls)
+            slot = 3 - a
+            pass_on(8, kvl.at[b], kvl.at[b], kr.at[b], dev(cls, mate(a), c)).start()
+            fan(9, cls, b, slot)
+            pass_on(
+                11, E.at[cls, slot], E.at[cls, slot], er.at[cls, slot], dev(cls, mate(a), c)
+            ).start()
+
+        @pl.when(i == 3)
+        def _():
+            a, c = axes(par)
+            fan(12, par, b, (a + 2) % 4)
+
+        @pl.when((i >= 4) & (i < 8))
+        def _():
+            cls = (i - 4) // 2
+            a, c = axes(cls)
+            pass_on(10 + i, kvl.at[b], kvl.at[b], kr.at[b], dev(cls, a, mate(c))).start()
+
     for load in loads[3:]:
         load.wait()
     gather = RingGather(wall.at[tp], wall, ws, wr)
     gather.begin()
+    for n in range(2):
+        turned = gt[n].T
+        for half in range(2):
+            G[z, y, half, n] = turned[64 * half : 64 * half + 64]
     upper = GridGather(G, Gs, Gr)
     lower = GridGather(D, Ds, Dr)
     upper.begin(0)
@@ -386,9 +470,12 @@
         M[t] = jnp.broadcast_to(m_new, (8, QW))
 
     def block(i, _):
-        o = i
-        b = ((z + 4 - o // 4) % 4) * 4 + (y + 4 - o % 4) % 4
-        pltpu.make_async_copy(ksrc.at[0], kvl.at[b], kr.at[b]).wait()
+        b = order(i)
+
+        @pl.when(i < 14)
+        def _():
+            arrive(i + 2)
+
         X[...] = kvl[b, 0:128, :].T
         g = kvl[b, 64:80, 0:128].astype(jnp.float32)
         bs = jnp.tile(g[4:5] + g[5:6] + g[6:7], (1, QW // 128))
@@ -418,8 +505,22 @@
             def _():
                 gather.stage(stage)
 
+        @pl.when(i == 6)
+        def _():
+            upper.relay(0)
+            lower.relay(0)
+
+        @pl.when(i == 8)
+        def _():
+            upper.finish(0)
+            upper.begin(1)
+            lower.finish(0)
+            lower.begin(1)
+
         return 0
 
+    arrive(0)
+    arrive(1)
     lax.fori_loop(0, 16, block, 0)
 
     head = tp * 4 + head_of(me)
@@ -447,6 +548,7 @@
             O[16 * t + n] = jnp.concatenate(
                 [heads[32 * n : 32 * n + 16], heads[32 * n + 16 : 32 * n + 32]], axis=1
             )
+    pl.semaphore_wait(line, 15)
     for t in range(NT):
         for u in range(2):
 
@@ -464,12 +566,7 @@
                 return 0
 
             lax.fori_loop(0, 8, send, 0)
-    upper.relay(0)
-    lower.relay(0)
-    upper.finish(0)
-    upper.begin(1)
-    lower.finish(0)
-    lower.begin(1)
+    upper.relay(1)
     gather.finish()
     pltpu.make_async_copy(att, att, gr).wait()
     for h in range(32):
@@ -484,7 +581,6 @@
     rows[tp] = layer_norm(p, gain1[...], bias1[...]).astype(jnp.bfloat16)
     spread = RingGather(rows.at[tp], rows, ns, nr)
     spread.begin()
-    upper.relay(1)
 
     x, core = tp // 2, tp % 2
     _, sibling, right, left, far = ring()
@@ -612,8 +708,8 @@
 
             lax.fori_loop(0, 8, sent, 0)
     gather.sent()
-    for copy in sends:
-        copy.wait_send()
+    for n in range(18):
+        pltpu.make_async_copy(ksrc.at[0], ksrc.at[0], ks.at[n]).wait()
     for to, copy in qsends:
 
         @pl.when(to != me)
@@ -654,9 +750,12 @@
         pltpu.VMEM((3, 96, 2048), bf),
         pltpu.VMEM((2, 48, 2048), bf),
         pltpu.VMEM((2, 96, 2048), bf),
-        dma((16,)), dma((16,)), dma((12,)), dma((12,)), dma((9,)), dma((8, 2)), dma((8,)),
+        pltpu.VMEM((2, 4, KVR, BL), bf),
+        pltpu.VMEM((2, 704, 128), bf),
+        dma((18,)), dma((16,)), dma((12,)), dma((12,)), dma((9,)), dma((8, 2)), dma((13,)),
         dma((96,)), dma, dma((2, 2, 4)), dma((2, 2, 4)), dma((2, 2, 4)), dma((2, 2, 4)),
-        dma((9,)), dma((8, 2)), dma((4,)), dma((4,)), dma((4,)), dma((4,)),
+        dma((9,)), dma((8, 2)), dma((4,)), dma((4,)), dma((4,)), dma((4,)), dma((2, 4)),
+        pltpu.SemaphoreType.REGULAR,
     ]
     return pl.pallas_call(
         layer_kernel,
@@ -693,9 +792,9 @@
         log_forget.T,
         out_weight,
         stream_in,
-        gate_weight.reshape(2, 64, 704),
-        up_weight.reshape(2, 64, 704),
-        down_weight.reshape(2, 2, 176, 128),
+        gate_weight.T,
+        up_weight.T,
+        down_weight,
         mix_gain[None],
         mix_bias[None],
         ffn_gain[None],

time: 164 us -> 143 us (0.87)
  Pallas kernels: 159 us -> 140 us
  local copies, waits for them, and re-layouts: 5.23 us -> 1.77 us
    pallas_call x1, Pallas kernels: 159 us -> 140 us  [layer(): pl.pallas_call(layer_kernel, name='layer', out_shape=jax.ShapeDtypeStruct...]
    unnamed x3 -> x1, local copies, waits for them, and re-layouts: 5.23 us -> 1.77 us
where the time goes in v5:
time: 143 us; the launch traced here: 142 us
  Pallas kernels  140 us (98%)
  local copies, waits for them, and re-layouts  1.77 us (1%)
    pallas_call x1, Pallas kernels, layer(): pl.pallas_call(layer_kernel, name='layer', out_shape=jax.ShapeDtypeStruct...  140 us

profile of v5, /device:TPU:0, one launch (start us, length us, event | category | flops | bytes accessed | tf_op | source)
XLA Modules:
  0.0 142.0 jit_solution(5148127557352258288)
XLA Ops:
  0.0 140.3 %layer.1 = bf16[96,2048]{1,0:T(8,128)(2,1)} custom-call(bf16[768,256]{1,0:T(8,128)(2,1)} %q_hbm.1, bf16[768,256]{1,0:T(8,128)(2,1)} %k_hbm.1, bf16[768,256]{1,0:T(8,128)(2,1)} %v_hbm.1, f32[4,768]{1,0:T(4,128)} %bitcast.9, bf16[256,2048]{1,0:T(8,128)(2,1)} %w_ref.1, bf16[768,2048]{1,0:T(8,128)(2,1)} %stream.1, bf16[704,128]{1,0:T(8,128)(2,1)} %bitcast.7, ...), custom_call_target="tpu_custom_call" | custom-call | tf_op jit(solution)/shard_map/layer/pallas_call | solution.py:760
  140.3 1.8 %copy.15 = bf16[96,2048]{1,0:T(8,128)(2,1)} copy(bf16[96,2048]{1,0:T(8,128)(2,1)} %layer.1) | data formatting | bytes 786432

commit v6 on v5

--- a/solution.py
+++ b/solution.py
@@ -13,7 +13,18 @@
 LOG2E = 1.4426950408889634
 NEG = -1e30
 BL = 768
-RELAY = (9, 10, 13)
+RELAY = (11, 12, 14)
+TURNS = (0, 4, 2, 3, 1, 8, 6, 5, 12, 7, 13, 10, 14, 9, 15, 11)
+AFTER = (
+    (0, (4,)),
+    (1, (1, 3, 2)),
+    (4, (6, 8)),
+    (6, (12, 7, 5)),
+    (9, (13, 10)),
+    (11, (14, 9)),
+    (13, (15,)),
+    (14, (11,)),
+)
 QW = 512
 NT = 6
 NB = 16
@@ -234,7 +245,7 @@
 def layer_kernel(
     q_hbm, k_hbm, v_hbm, g_ref, w_ref, stream, gate_w, up_w, down_w, gain1, bias1, gain2, bias2,
     out,
-    q_ref, k_ref, v_ref, att, wall, kvl, qt, ksrc, qsrc, X, R, S0, S1, mx0, mx1, M, A, O,
+    q_ref, k_ref, v_ref, att, wall, kvl, qt, ksrc, qsrc, X, R, S0, S1, S2, S3, mx0, mx1, mx2, mx3, M, A, O,
     G, D, rows, lhs, res, hid, pb, sib, zz, rel, inn, E, gt,
     ks, kr, qs, qr, ws, wr, ld, gs, gr, Gs, Gr, Ds, Dr, ns, nr, ss, sr, hs, hr, er, line,
 ):
@@ -364,64 +375,56 @@
         pass_on(n, E.at[cls, slot], kvl.at[b], kr.at[b], dev(cls, a, 3 - c)).start()
         pass_on(n + 1, kvl.at[b], kvl.at[b], kr.at[b], dev(cls, a, mate(c))).start()
 
-    def order(i):
-        j = jnp.maximum(i - 4, 0)
-        g, cls, f = j // 4, j % 4 // 2, j % 2
-        a, c = axes(cls)
-        far_c = jnp.where(g == 0, 3 - c, jnp.where(g == 1, mate(c), (c + 2) % 4))
-        late = dev(cls, (cls + far_c) % 2 + 2 * f, far_c)
-        ya, yc = axes(1 - par)
-        xa, xc = axes(par)
-        early = jnp.where(
-            i < 2,
-            jnp.where(i == 0, me, dev(1 - par, mate(ya), yc)),
-            jnp.where(i == 2, dev(1 - par, 3 - ya, yc), dev(par, (xa + 2) % 4, xc)),
-        )
-        return jnp.where(i < 4, early, late)
-
-    def arrive(i):
-        b = order(i)
+    X_, Y_ = par, 1 - par
+    xa, xc = axes(X_)
+    ya, yc = axes(Y_)
+    blocks = (
+        me,
+        dev(Y_, mate(ya), yc),
+        dev(Y_, 3 - ya, yc),
+        dev(Y_, ya, 3 - yc),
+        dev(Y_, ya, mate(yc)),
+        dev(X_, (xa + 2) % 4, xc),
+        dev(X_, mate(xa), 3 - xc),
+        dev(X_, 3 - xa, 3 - xc),
+        dev(X_, mate(xa), mate(xc)),
+        dev(X_, 3 - xa, mate(xc)),
+        dev(Y_, (ya + 2) % 4, 3 - yc),
+        dev(Y_, (ya + 2) % 4, mate(yc)),
+        dev(X_, xa, (xc + 2) % 4),
+        dev(Y_, mate(ya), (yc + 2) % 4),
+        dev(Y_, 3 - ya, (yc + 2) % 4),
+        dev(X_, (xa + 2) % 4, (xc + 2) % 4),
+    )
+
+    def arrive(n):
+        b = blocks[n]
         pltpu.make_async_copy(ksrc.at[0], kvl.at[b], kr.at[b]).wait()
-
-        @pl.when(i == 1)
-        def _():
-            a, c = axes(1 - par)
-            fan(6, 1 - par, b, mate(a))
-
-        @pl.when(i == 2)
-        def _():
-            cls = 1 - par
-            a, c = axes(cls)
-            slot = 3 - a
-            pass_on(8, kvl.at[b], kvl.at[b], kr.at[b], dev(cls, mate(a), c)).start()
-            fan(9, cls, b, slot)
-            pass_on(
-                11, E.at[cls, slot], E.at[cls, slot], er.at[cls, slot], dev(cls, mate(a), c)
-            ).start()
-
-        @pl.when(i == 3)
-        def _():
-            a, c = axes(par)
-            fan(12, par, b, (a + 2) % 4)
-
-        @pl.when((i >= 4) & (i < 8))
-        def _():
-            cls = (i - 4) // 2
-            a, c = axes(cls)
-            pass_on(10 + i, kvl.at[b], kvl.at[b], kr.at[b], dev(cls, a, mate(c))).start()
+        block = kvl.at[b]
+        if n == 1:
+            fan(6, Y_, b, mate(ya))
+        if n == 2:
+            slot = 3 - ya
+            to = dev(Y_, mate(ya), yc)
+            pass_on(8, block, block, kr.at[b], to).start()
+            fan(9, Y_, b, slot)
+            pass_on(11, E.at[Y_, slot], E.at[Y_, slot], er.at[Y_, slot], to).start()
+        if n == 5:
+            fan(12, X_, b, (xa + 2) % 4)
+        if n in (3, 10):
+            pass_on(14 + n // 10, block, block, kr.at[b], dev(Y_, ya, mate(yc))).start()
+        if n in (6, 7):
+            pass_on(10 + n, block, block, kr.at[b], dev(X_, xa, mate(xc))).start()
 
     for load in loads[3:]:
         load.wait()
     gather = RingGather(wall.at[tp], wall, ws, wr)
-    gather.begin()
     for n in range(2):
         turned = gt[n].T
         for half in range(2):
             G[z, y, half, n] = turned[64 * half : 64 * half + 64]
     upper = GridGather(G, Gs, Gr)
     lower = GridGather(D, Ds, Dr)
-    upper.begin(0)
-    lower.begin(0)
 
     row = lax.broadcasted_iota(jnp.int32, (64, QW), 0)
     ones = jnp.where((row >= 1) & (row < 4), 1.0, 0.0).astype(jnp.bfloat16)
@@ -439,8 +442,8 @@
         A[t] = jnp.zeros((80, QW), jnp.float32)
 
     mm = member_of(me)
-    S = (S0, S1)
-    mx = (mx0, mx1)
+    S = (S0, S1, S2, S3)
+    mx = (mx0, mx1, mx2, mx3)
 
     def qk(t, n):
         x = X[...]
@@ -470,11 +473,9 @@
         M[t] = jnp.broadcast_to(m_new, (8, QW))
 
     def block(i, _):
-        b = order(i)
-
-        @pl.when(i < 14)
-        def _():
-            arrive(i + 2)
+        b = blocks[TURNS[0]]
+        for n in range(1, 16):
+            b = jnp.where(i == n, blocks[TURNS[n]], b)
 
         X[...] = kvl[b, 0:128, :].T
         g = kvl[b, 64:80, 0:128].astype(jnp.float32)
@@ -483,21 +484,48 @@
         def live(t):
             return chunk_of(t, mm) * QW + QW > b * BL
 
-        for t in range(NT):
-            first = live(t) if t == 0 else live(t) & jnp.logical_not(live(t - 1))
-
-            @pl.when(first)
+        def ready(t):
+            for n in (t, t + 1):
+                if n < NT:
+                    qk(n, n % 4)
+
+        def masks(t):
+            for n in (t, t + 1):
+                if n < NT:
+                    mask(b, n, n % 4)
+
+        for t in range(0, NT, 2):
+
+            @pl.when(live(t) if t == 0 else live(t) & jnp.logical_not(live(t - 1)))
             def _():
-                qk(t, t % 2)
-                mask(b, t, t % 2)
+                ready(t)
+                masks(t)
 
             @pl.when(live(t))
             def _():
-                if t + 1 < NT:
-                    qk(t + 1, (t + 1) % 2)
-                pv(b, t, t % 2, bs)
-                if t + 1 < NT:
-                    mask(b, t + 1, (t + 1) % 2)
+                ready(t + 2)
+                pv(b, t, t % 4, bs)
+                pv(b, t + 1, (t + 1) % 4, bs)
+                masks(t + 2)
+
+            @pl.when(live(t + 1) & jnp.logical_not(live(t)))
+            def _():
+                qk(t + 1, (t + 1) % 4)
+                mask(b, t + 1, (t + 1) % 4)
+                ready(t + 2)
+                pv(b, t + 1, (t + 1) % 4, bs)
+                masks(t + 2)
+
+        for n, arrivals in AFTER:
+
+            @pl.when(i == n)
+            def _():
+                for k in arrivals:
+                    arrive(k)
+
+        @pl.when(i == 1)
+        def _():
+            gather.begin()
 
         for stage in range(3):
 
@@ -505,22 +533,24 @@
             def _():
                 gather.stage(stage)
 
-        @pl.when(i == 6)
+        @pl.when(i == 5)
+        def _():
+            upper.begin(0)
+            lower.begin(0)
+
+        @pl.when(i == 8)
         def _():
             upper.relay(0)
             lower.relay(0)
 
-        @pl.when(i == 8)
+        @pl.when(i == 10)
         def _():
             upper.finish(0)
             upper.begin(1)
-            lower.finish(0)
-            lower.begin(1)
 
         return 0
 
     arrive(0)
-    arrive(1)
     lax.fori_loop(0, 16, block, 0)
 
     head = tp * 4 + head_of(me)
@@ -566,6 +596,8 @@
                 return 0
 
             lax.fori_loop(0, 8, send, 0)
+    lower.finish(0)
+    lower.begin(1)
     upper.relay(1)
     gather.finish()
     pltpu.make_async_copy(att, att, gr).wait()
@@ -734,6 +766,10 @@
         pltpu.VMEM((NT, 256, QW), bf),
         pltpu.VMEM((BL, QW), jnp.float32),
         pltpu.VMEM((BL, QW), jnp.float32),
+        pltpu.VMEM((BL, QW), jnp.float32),
+        pltpu.VMEM((BL, QW), jnp.float32),
+        pltpu.VMEM((8, QW), jnp.float32),
+        pltpu.VMEM((8, QW), jnp.float32),
         pltpu.VMEM((8, QW), jnp.float32),
         pltpu.VMEM((8, QW), jnp.float32),
         pltpu.VMEM((NT, 8, QW), jnp.float32),

time: 143 us -> 138 us (0.965)
  Pallas kernels: 140 us -> 135 us
    pallas_call x1, Pallas kernels: 140 us -> 135 us  [layer(): pl.pallas_call(layer_kernel, name='layer', out_shape=jax.ShapeDtypeStruct...]
where the time goes in v6:
time: 138 us; the launch traced here: 137 us
  Pallas kernels  135 us (98%)
  local copies, waits for them, and re-layouts  1.77 us (1%)
    pallas_call x1, Pallas kernels, layer(): pl.pallas_call(layer_kernel, name='layer', out_shape=jax.ShapeDtypeStruct...  135 us

profile of v6, /device:TPU:0, one launch (start us, length us, event | category | flops | bytes accessed | tf_op | source)
XLA Modules:
  0.0 136.6 jit_solution(4740973091530125227)
XLA Ops:
  0.0 134.8 %layer.1 = bf16[96,2048]{1,0:T(8,128)(2,1)} custom-call(bf16[768,256]{1,0:T(8,128)(2,1)} %q_hbm.1, bf16[768,256]{1,0:T(8,128)(2,1)} %k_hbm.1, bf16[768,256]{1,0:T(8,128)(2,1)} %v_hbm.1, f32[4,768]{1,0:T(4,128)} %bitcast.9, bf16[256,2048]{1,0:T(8,128)(2,1)} %w_ref.1, bf16[768,2048]{1,0:T(8,128)(2,1)} %stream.1, bf16[704,128]{1,0:T(8,128)(2,1)} %bitcast.7, ...), custom_call_target="tpu_custom_call" | custom-call | tf_op jit(solution)/shard_map/layer/pallas_call | solution.py:796
  134.8 1.8 %copy.15 = bf16[96,2048]{1,0:T(8,128)(2,1)} copy(bf16[96,2048]{1,0:T(8,128)(2,1)} %layer.1) | data formatting | bytes 786432
